TPU v7x, 128 devices: a whole 4x4x4 slice. The times are simulated.
128 devices in a mesh: fs: 16 (over z, y), tp: 8 (over x, core).
Axes of the slice: x: 4, y: 4, z: 4, core: 2. Of those that a mesh axis runs over, the one named last changes fastest.
Arguments:
- tokens: bfloat16 [16384, 2048], P('fs'), may hold values from -6 to 6
- w_gate_side: bfloat16 [2048, 1024], P('fs', 'tp'), may hold values from -0.125 to 0.125
- w_value_side: bfloat16 [2048, 1024], P('fs', 'tp'), may hold values from -0.125 to 0.125
- spatial_gain: float32 [1024], P('tp'), may hold values from 0.1 to 1.9
- w_spatial: bfloat16 [16, 128, 128], P('tp'), may hold values from -0.5 to 0.5
- spatial_bias: float32 [16, 128], P('tp'), may hold values from 0.1 to 1.9
- w_mixer_out: bfloat16 [1024, 2048], P('tp', 'fs'), may hold values from -0.1875 to 0.1875
- first_gain: float32 [2048], replicated, may hold values from 0.1 to 1.9
- w_ff_gate: bfloat16 [2048, 5632], P('fs', 'tp'), may hold values from -0.125 to 0.125
- w_ff_up: bfloat16 [2048, 5632], P('fs', 'tp'), may hold values from -0.125 to 0.125
- conv_gate_taps: float32 [3, 5632], P(None, 'tp'), may hold values from -3.5 to 3.5
- conv_up_taps: float32 [3, 5632], P(None, 'tp'), may hold values from -3.5 to 3.5
- w_ff_down: bfloat16 [5632, 2048], P('tp', 'fs'), may hold values from -0.078125 to 0.078125
- second_gain: float32 [2048], replicated, may hold values from 0.1 to 1.9
Outputs:
- layer_out: bfloat16 [16384, 2048], P('fs', 'tp')
All inputs are finite; a program needn't handle non-finite values.
Results may differ from a plain program's by a relative error of at most 0.015.
Values may be sent and summed in bfloat16 or wider, within the bound.
A program may use at most 64 MiB of HBM per device.

v0:
```python
import jax
import jax.numpy as jnp
from jax import lax
from jax.sharding import Mesh
from jax.sharding import PartitionSpec as P

D = 2048
GROUP_DIM = 64
SG_WIDTH = 1024
SPAN = 128
SEQ = 256
FS = ("fs_0", "fs_1")


residual_scale = 2.0**0.25
norm_eps = 1e-05


def sent_to_all(array, axis):
    devices = lax.axis_size(axis)
    return lax.all_to_all(
        jnp.broadcast_to(array[None], (devices, *array.shape)), axis, 0, 0, tiled=True
    )


def over_copies(array, axis):
    everything = sent_to_all(array, axis)
    return jnp.sum(everything, axis=0)


def packed_total(arrays, axis):
    ends = [0]
    for a in arrays:
        ends.append(ends[-1] + a.size)
    so_far = over_copies(jnp.concatenate([a.ravel() for a in arrays]), axis)
    return tuple((so_far[b:e].reshape(a.shape) for a, b, e in zip(arrays, ends, ends[1:])))


def in_one_piece(arrays, axis, dim, along):
    ends, at = ([], 0)
    for a in arrays[:-1]:
        at += a.shape[along]
        ends.append(at)
    both = jnp.concatenate(arrays, axis=along)
    return tuple(jnp.split(lax.all_gather(both, axis, axis=dim, tiled=True), ends, axis=along))


def whole_of(array, axes, dim):
    filled = array
    for number in range(len(axes) - 1, -1, -1):
        filled = lax.all_gather(filled, axes[number], axis=dim, tiled=True)
    return filled


def split_norm(values, gain, width):
    sums = packed_total((jnp.sum(values, axis=1), jnp.sum(values * values, axis=1)), "tp")
    mean = sums[0][:, None] / width
    spread = sums[1][:, None] / width - mean * mean
    return (values - mean) * lax.rsqrt(spread + norm_eps) * gain


def whole_norm(values, gain):
    width = values.shape[-1]
    mean = jnp.sum(values, axis=-1, keepdims=True) / width
    spread = jnp.sum(values * values, axis=-1, keepdims=True) / width - mean * mean
    return (values - mean) * lax.rsqrt(spread + norm_eps) * gain


def causal_taps(pre, taps):
    count = pre.shape[0] // SEQ
    blocks = pre.reshape(count, SEQ, pre.shape[1])
    padded = jnp.pad(blocks, ((0, 0), (2, 0), (0, 0)))
    result = padded[:, 0:SEQ] * taps[0] + padded[:, 1 : SEQ + 1] * taps[1] + padded[:, 2:] * taps[2]
    return result.reshape(pre.shape)


def add_rows(left, piece):
    return jnp.dot(left, piece, preferred_element_type=jnp.float32)


def per_device(
    tokens,
    w_gate_side,
    w_value_side,
    spatial_gain,
    w_spatial,
    spatial_bias,
    w_mixer_out,
    first_gain,
    w_ff_gate,
    w_ff_up,
    conv_gate_taps,
    conv_up_taps,
    w_ff_down,
    second_gain,
):
    rows = tokens.shape[0]
    width_dev = D // lax.axis_size("tp")
    offset = lax.axis_index("tp") * width_dev
    pieces = (
        lax.all_gather(w_gate_side, FS, axis=0, tiled=True),
        lax.all_gather(w_value_side, FS, axis=0, tiled=True),
    )
    gate_pre = add_rows(tokens, pieces[0])
    value_pre = add_rows(tokens, pieces[1])
    gate_act = jax.nn.gelu(gate_pre)
    value_norm = split_norm(jax.nn.gelu(value_pre), spatial_gain, SG_WIDTH).astype(jnp.bfloat16)
    groups_dev = w_spatial.shape[0]
    blocks = value_norm.reshape(rows // SPAN, SPAN, groups_dev, GROUP_DIM)
    lower = jnp.tril(jnp.ones((SPAN, SPAN), jnp.bool_))
    causal_w = jnp.where(lower[None], w_spatial, jnp.zeros_like(w_spatial))
    mixed = jnp.einsum("gts,nsgc->ntgc", causal_w, blocks, preferred_element_type=jnp.float32)
    mixed = mixed + spatial_bias.T[None, :, :, None]
    spatial_out = (gate_act * mixed.reshape(rows, groups_dev * GROUP_DIM)).astype(jnp.bfloat16)
    mixer_part = jnp.dot(
        spatial_out,
        lax.all_gather(w_mixer_out, FS, axis=1, tiled=True),
        preferred_element_type=jnp.float32,
    )
    mixer_sum = lax.psum(mixer_part.astype(jnp.bfloat16), "tp").astype(jnp.float32)
    first_whole = whole_norm(
        residual_scale * tokens.astype(jnp.float32) + mixer_sum, first_gain
    ).astype(jnp.bfloat16)
    first_own = lax.dynamic_slice_in_dim(first_whole, offset, width_dev, 1)
    pieces = in_one_piece((w_ff_gate, w_ff_up), FS, 0, 1)
    ff_gate_pre = add_rows(first_whole, pieces[0])
    ff_up_pre = add_rows(first_whole, pieces[1])
    ff_gate = causal_taps(ff_gate_pre, conv_gate_taps)
    ff_up = causal_taps(ff_up_pre, conv_up_taps)
    ff_hidden = (jax.nn.silu(ff_gate) * ff_up).astype(jnp.bfloat16)
    ff_part = jnp.dot(ff_hidden, whole_of(w_ff_down, FS, 1), preferred_element_type=jnp.float32)
    ff_sum = lax.psum_scatter(
        ff_part.astype(jnp.bfloat16), "tp", scatter_dimension=1, tiled=True
    ).astype(jnp.float32)
    own_second = lax.dynamic_slice_in_dim(second_gain, offset, width_dev, 0)
    layer_out = split_norm(residual_scale * first_own.astype(jnp.float32) + ff_sum, own_second, D)
    return layer_out.astype(jnp.bfloat16)


def solution(mesh):
    finer = Mesh(mesh.devices.reshape(4, 4, mesh.shape["tp"]), ("fs_0", "fs_1", "tp"))
    in_specs = (
        P(FS, None),
        P(FS, "tp"),
        P(FS, "tp"),
        P("tp"),
        P("tp", None, None),
        P("tp", None),
        P("tp", FS),
        P(),
        P(FS, "tp"),
        P(FS, "tp"),
        P(None, "tp"),
        P(None, "tp"),
        P("tp", FS),
        P(),
    )
    out_specs = P(FS, "tp")
    return jax.shard_map(
        per_device, mesh=finer, in_specs=in_specs, out_specs=out_specs, check_vma=False
    )
```

profile of v0, /device:TPU:1, one launch (start us, length us, event | category | flops | bytes accessed | tf_op | source)
XLA Modules:
  0.0 286.0 jit_solution(8457939443440648281)
XLA Ops:
  7.4 21.1 %all_gather.19 = bf16[2048,128]{1,0:T(8,128)(2,1)S(1)} all-gather(bf16[128,128]{1,0:T(8,128)(2,1)} %param.16), channel_id=1, replica_groups=mesh['fs_0'=4,'fs_1'=4,'tp'=8] {'fs_0','fs_1'}, dimensions={0}, use_global_device_ids=true | all-gather | bytes 557056 | tf_op jit(solution)/shard_map/all_gather | solution.py:102
  28.5 0.0 copy-start.9
  28.5 0.0 copy-start.14
  28.5 3.6 %fusion.54 = (f32[1024]{0:T(1024)S(1)}, f32[1024]{0:T(1024)S(1)}, f32[1024,128]{1,0:T(8,128)S(1)}) fusion(bf16[1024,2048]{1,0:T(8,128)(2,1)} %param.14, bf16[2048,128]{1,0:T(8,128)(2,1)S(1)} %all_gather.19), kind=kOutput, calls=%fused_computation.87 | convolution fusion | flops 538310656 | bytes 5251072 | tf_op jit(solution)/shard_map/dot_general | solution.py:78
  32.2 0.7 broadcast_in_dim.13
  32.8 10.2 %all-to-all-start = ((f32[8,1,2048]{2,1,0:T(1,128)}), f32[8,1,2048]{2,1,0:T(1,128)S(1)}, u32[]{:S(2)}, u32[]{:S(2)}) async-start(f32[8,1,2048]{2,1,0:T(1,128)} %broadcast_in_dim.13), calls=%async_computation | async-start | bytes 131072 | tf_op jit(solution)/shard_map/all_to_all | solution.py:21
  43.0 18.7 %all_gather.18 = bf16[2048,128]{1,0:T(8,128)(2,1)S(1)} all-gather(bf16[128,128]{1,0:T(8,128)(2,1)S(1)} %copy-done.8), channel_id=1, replica_groups=mesh['fs_0'=4,'fs_1'=4,'tp'=8] {'fs_0','fs_1'}, dimensions={0}, use_global_device_ids=true | all-gather | bytes 557056 | tf_op jit(solution)/shard_map/all_gather | solution.py:101
  61.7 17.1 %all_gather.20 = bf16[128,2048]{1,0:T(8,128)(2,1)S(1)} all-gather(bf16[128,128]{1,0:T(8,128)(2,1)S(1)} %copy-done.9), channel_id=1, replica_groups=mesh['fs_0'=4,'fs_1'=4,'tp'=8] {'fs_0','fs_1'}, dimensions={1}, use_global_device_ids=true | all-gather | bytes 557056 | tf_op jit(solution)/shard_map/all_gather | solution.py:117
  78.8 0.1 reduce_sum.74
  78.9 0.3 multiply_convert_fusion.4
  79.3 0.2 reshape.88
  79.5 0.3 fusion.14
  79.8 0.6 copy.55
  80.4 0.6 reshape.89
  81.0 8.5 %convolution_convert_fusion.1 = bf16[1024,2048]{1,0:T(8,128)(2,1)} fusion(bf16[128,2048]{1,0:T(8,128)(2,1)S(1)} %all_gather.20, f32[1024,128]{1,0:T(8,128)S(1)} %reshape.89, bf16[1024,2048]{1,0:T(8,128)(2,1)} %param.14, bf16[2048,128]{1,0:T(8,128)(2,1)S(1)} %all_gather.18), kind=kOutput, calls=%fused_computation.9 | convolution fusion | flops 1077149696 | bytes 9961472 | tf_op jit(solution)/shard_map/dot_general | solution.py:115
  89.5 0.0 all-reduce.4.cloned.1.call-update
  89.6 0.0 all-gather.3.cloned.1.call-start
  89.6 0.8 copy-done.5
  90.4 0.1 copy-done.6
  90.5 0.8 pad_maximum_fusion
  91.3 0.0 all-gather.3.cloned.1.call-update
  91.3 0.0 all-gather.5.cloned.1.call-start
  91.4 10.9 %all_gather.22 = bf16[704,512]{1,0:T(8,128)(2,1)} all-gather(bf16[704,128]{1,0:T(8,128)(2,1)S(1)} %copy-done.4), channel_id=1, replica_groups=mesh['fs_0'=4,'fs_1'=4,'tp'=8] {'fs_1'}, dimensions={1}, use_global_device_ids=true | all-gather | bytes 901120 | tf_op jit(solution)/shard_map/all_gather | solution.py:51
  102.3 0.0 all-gather.5.cloned.1.call-update
  102.3 0.2 reduce-scatter.2.cloned.1.call-start
  102.7 67.8 %all-reduce.4.cloned.1.call-done = bf16[1024,2048]{1,0:T(8,128)(2,1)} async-done(((bf16[1024,2048]{1,0:T(8,128)(2,1)}), bf16[1024,2048]{1,0:T(8,128)(2,1)}) %all-reduce.4.cloned.1.call-update) | async-done | bytes 4194320 | tf_op jit(solution)/shard_map/psum | solution.py:120
  170.5 5.1 %fusion = (f32[1024]{0:T(1024)S(1)}, f32[1024]{0:T(1024)S(1)}) fusion(bf16[1024,2048]{1,0:T(8,128)(2,1)} %all-reduce.4.cloned.1.call-done, bf16[1024,2048]{1,0:T(8,128)(2,1)} %param.14), kind=kLoop, calls=%fused_computation.3 | loop fusion | flops 14678016 | bytes 8396800 | tf_op jit(solution)/shard_map/reduce_sum | solution.py:64
  175.6 1.1 copy-done.1
  176.7 3.6 %multiply_convert_fusion = bf16[1024,2048]{1,0:T(8,128)(2,1)} fusion(bf16[1024,2048]{1,0:T(8,128)(2,1)S(1)} %copy-done.1, bf16[1024,2048]{1,0:T(8,128)(2,1)S(1)} %copy-done, f32[2048]{0:T(1024)S(1)} %copy-done.10, f32[1024]{0:T(1024)S(1)} %get-tuple-element.22, f32[1024]{0:T(1024)S(1)} %get-tuple-element.21), kind=kLoop, calls=%fused_computation | loop fusion | flops 16777216 | bytes 12599296 | tf_op jit(solution)/shard_map/convert_element_type | solution.py:123
  180.3 7.8 %fusion.11 = f32[1024,704]{0,1:T(8,128)} fusion(bf16[1024,2048]{1,0:T(8,128)(2,1)} %multiply_convert_fusion, bf16[2048,1408]{0,1:T(8,128)(2,1)} %all-gather.3.cloned.1.call-done), kind=kOutput, calls=%fused_computation.20 | convolution fusion | flops 2952790016 | bytes 9961472 | tf_op jit(solution)/shard_map/dot_general | solution.py:78
  188.1 3.2 %reshape.83 = f32[4,256,704]{1,0,2:T(4,128)S(1)} reshape(f32[1024,704]{0,1:T(8,128)} %fusion.11) | data formatting | bytes 5767168 | tf_op jit(solution)/shard_map/reshape | solution.py:71
  191.4 5.8 %fusion.3 = f32[4,256,704]{1,0,2:T(4,128)S(1)} fusion(f32[4,256,704]{1,0,2:T(4,128)S(1)} %reshape.83, f32[704]{0:T(1024)S(1)} %get-tuple-element.12, f32[704]{0:T(1024)S(1)} %get-tuple-element.13, f32[704]{0:T(1024)S(1)} %get-tuple-element.11), kind=kLoop, calls=%fused_computation.12 | loop fusion | flops 3604480 | bytes 5775616 | tf_op jit(solution)/shard_map/add | solution.py:73
  197.3 2.2 copy.63
  199.5 1.0 copy-done.2
  200.5 4.8 %fusion.9 = f32[1024,704]{0,1:T(8,128)} fusion(bf16[1024,2048]{1,0:T(8,128)(2,1)S(1)} %copy-done.2, bf16[2048,1408]{0,1:T(8,128)(2,1)S(1)} %copy-done.15), kind=kOutput, calls=%fused_computation.18 | convolution fusion | flops 2952790016 | bytes 9961472 | tf_op jit(solution)/shard_map/dot_general | solution.py:78
  205.3 3.2 %reshape.85 = f32[4,256,704]{1,0,2:T(4,128)S(1)} reshape(f32[1024,704]{0,1:T(8,128)} %fusion.9) | data formatting | bytes 5767168 | tf_op jit(solution)/shard_map/reshape | solution.py:71
  208.5 6.1 %fusion.7 = f32[4,256,704]{1,0,2:T(4,128)S(1)} fusion(f32[4,256,704]{1,0,2:T(4,128)S(1)} %reshape.85, f32[704]{0:T(1024)S(1)} %get-tuple-element.15, f32[704]{0:T(1024)S(1)} %get-tuple-element.16, f32[704]{0:T(1024)S(1)} %get-tuple-element.14), kind=kLoop, calls=%fused_computation.16 | loop fusion | flops 3604480 | bytes 5775616 | tf_op jit(solution)/shard_map/add | solution.py:73
  214.7 2.3 copy.64
  217.0 8.3 %convolution_convert_fusion = bf16[1024,2048]{1,0:T(8,128)(2,1)} fusion(bf16[704,2048]{1,0:T(8,128)(2,1)} %all-gather.5.cloned.1.call-done, f32[1024,704]{0,1:T(8,128)} %bitcast.33, f32[1024,704]{0,1:T(8,128)S(1)} %bitcast.32), kind=kOutput, calls=%fused_computation.8 | convolution fusion | flops 2959212544 | bytes 12845056 | tf_op jit(solution)/shard_map/dot_general | solution.py:131
  225.3 0.0 reduce-scatter.2.cloned.1.call-update
  225.3 36.9 %reduce-scatter.2.cloned.1.call-done = bf16[1024,256]{1,0:T(8,128)(2,1)} async-done(((bf16[1024,2048]{1,0:T(8,128)(2,1)}), bf16[1024,256]{1,0:T(8,128)(2,1)}) %reduce-scatter.2.cloned.1.call-update) | async-done | bytes 524304 | tf_op jit(solution)/shard_map/reduce_scatter | solution.py:132
  262.2 1.6 fusion.15
  263.8 0.7 broadcast_in_dim.19
  264.4 6.8 %all-to-all-start.1 = ((f32[8,1,2048]{2,1,0:T(1,128)}), f32[8,1,2048]{2,1,0:T(1,128)S(1)}, u32[]{:S(2)}, u32[]{:S(2)}) async-start(f32[8,1,2048]{2,1,0:T(1,128)} %broadcast_in_dim.19), calls=%async_computation.2 | async-start | bytes 131072 | tf_op jit(solution)/shard_map/all_to_all | solution.py:21
  271.3 0.8 dynamic_slice.7
  272.1 4.1 %all-to-all-done.1 = f32[8,1,2048]{2,1,0:T(1,128)S(1)} async-done(((f32[8,1,2048]{2,1,0:T(1,128)}), f32[8,1,2048]{2,1,0:T(1,128)S(1)}, u32[]{:S(2)}, u32[]{:S(2)}) %all-to-all-start.1) | async-done | bytes 65568 | tf_op jit(solution)/shard_map/all_to_all | solution.py:21
  276.2 0.1 reduce_sum.79
  276.2 2.3 multiply_convert_fusion.3
  (38 shorter events, 0.2 us)
Async XLA Ops:
  28.5 14.5 %copy-start.8 = (bf16[128,128]{1,0:T(8,128)(2,1)S(1)}, bf16[128,128]{1,0:T(8,128)(2,1)}, u32[]{:S(2)}) copy-start(bf16[128,128]{1,0:T(8,128)(2,1)} %param.15) | copy-start | bytes 98308
  28.5 33.2 %copy-start.9 = (bf16[128,128]{1,0:T(8,128)(2,1)S(1)}, bf16[128,128]{1,0:T(8,128)(2,1)}, u32[]{:S(2)}) copy-start(bf16[128,128]{1,0:T(8,128)(2,1)} %param.20) | copy-start | bytes 98308
  28.5 50.4 %copy-start.14 = (f32[128]{0:T(128)S(1)}, f32[128]{0:T(128)}, u32[]{:S(2)}) copy-start(f32[128]{0:T(128)} %param.17) | copy-start | bytes 1540
  28.5 51.0 %copy-start.7 = (bf16[2,128,128]{2,1,0:T(8,128)(2,1)S(1)}, bf16[2,128,128]{2,1,0:T(8,128)(2,1)}, u32[]{:S(2)}) copy-start(bf16[2,128,128]{2,1,0:T(8,128)(2,1)} %param.18) | copy-start | bytes 196612
  28.5 51.0 %copy-start.13 = (f32[2,128]{1,0:T(2,128)S(1)}, f32[2,128]{1,0:T(2,128)}, u32[]{:S(2)}) copy-start(f32[2,128]{1,0:T(2,128)} %param.19) | copy-start | bytes 3076
  32.8 46.0 %all-to-all-start = ((f32[8,1,2048]{2,1,0:T(1,128)}), f32[8,1,2048]{2,1,0:T(1,128)S(1)}, u32[]{:S(2)}, u32[]{:S(2)}) async-start(f32[8,1,2048]{2,1,0:T(1,128)} %broadcast_in_dim.13), calls=%async_computation | async-start | bytes 131072 | tf_op jit(solution)/shard_map/all_to_all | solution.py:21
  43.0 127.4 %all-reduce.4.cloned.1.call-start = ((), (), s32[]{:S(2)}) async-start(), calls=%async_computation.3 | async-start | bytes 8388608 | tf_op jit(solution)/shard_map/psum | solution.py:120
  89.5 0.9 copy-start.5
  89.5 1.0 copy-start.6
  89.5 1.8 copy-start.4
  89.5 13.0 %copy-start.11 = (f32[3,704]{1,0:T(4,128)S(1)}, f32[3,704]{1,0:T(4,128)}, u32[]{:S(2)}) copy-start(f32[3,704]{1,0:T(4,128)} %param.24) | copy-start | bytes 25348
  89.5 13.1 %copy-start.12 = (f32[3,704]{1,0:T(4,128)S(1)}, f32[3,704]{1,0:T(4,128)}, u32[]{:S(2)}) copy-start(f32[3,704]{1,0:T(4,128)} %param.25) | copy-start | bytes 25348
  89.6 90.8 %all-gather.3.cloned.1.call-start = ((), (), s32[]{:S(2)}) async-start(), calls=%async_computation.4 | async-start | bytes 6127616 | tf_op jit(solution)/shard_map/all_gather | solution.py:45
  91.3 125.7 %all-gather.5.cloned.1.call-start = ((), (), s32[]{:S(2)}) async-start(), calls=%async_computation.5 | async-start | bytes 3604480 | tf_op jit(solution)/shard_map/all_gather | solution.py:51
  102.3 159.9 %reduce-scatter.2.cloned.1.call-start = ((), (), s32[]{:S(2)}) async-start(), calls=%async_computation.6 | async-start | bytes 4718592 | tf_op jit(solution)/shard_map/reduce_scatter | solution.py:132
  102.7 72.9 %copy-start.10 = (f32[2048]{0:T(1024)S(1)}, f32[2048]{0:T(1024)}, u32[]{:S(2)}) copy-start(f32[2048]{0:T(1024)} %param.21) | copy-start | bytes 24580
  170.5 5.1 %copy-start = (bf16[1024,2048]{1,0:T(8,128)(2,1)S(1)}, bf16[1024,2048]{1,0:T(8,128)(2,1)}, u32[]{:S(2)}) copy-start(bf16[1024,2048]{1,0:T(8,128)(2,1)} %param.14) | copy-start | bytes 12582916
  170.5 6.2 %copy-start.1 = (bf16[1024,2048]{1,0:T(8,128)(2,1)S(1)}, bf16[1024,2048]{1,0:T(8,128)(2,1)}, u32[]{:S(2)}) copy-start(bf16[1024,2048]{1,0:T(8,128)(2,1)} %all-reduce.4.cloned.1.call-done) | copy-start | bytes 12582916
  191.4 8.1 %copy-start.15 = (bf16[2048,1408]{0,1:T(8,128)(2,1)S(1)}, bf16[2048,1408]{0,1:T(8,128)(2,1)}, u32[]{:S(2)}) copy-start(bf16[2048,1408]{0,1:T(8,128)(2,1)} %all-gather.3.cloned.1.call-done) | copy-start | bytes 17301508
  197.3 3.2 %copy-start.2 = (bf16[1024,2048]{1,0:T(8,128)(2,1)S(1)}, bf16[1024,2048]{1,0:T(8,128)(2,1)}, u32[]{:S(2)}) copy-start(bf16[1024,2048]{1,0:T(8,128)(2,1)} %multiply_convert_fusion) | copy-start | bytes 12582916
  214.7 2.3 copy-start.3
  264.4 11.7 %all-to-all-start.1 = ((f32[8,1,2048]{2,1,0:T(1,128)}), f32[8,1,2048]{2,1,0:T(1,128)S(1)}, u32[]{:S(2)}, u32[]{:S(2)}) async-start(f32[8,1,2048]{2,1,0:T(1,128)} %broadcast_in_dim.19), calls=%async_computation.2 | async-start | bytes 131072 | tf_op jit(solution)/shard_map/all_to_all | solution.py:21
Sparse Core Ops, SparseCore 0:
  89.7 80.7 all-reduce.3
  225.4 36.7 reduce-scatter.1
Sparse Core Ops, SparseCore 1:
  92.2 72.0 all-gather.2
  165.7 37.8 all-gather.4
where the time goes:
time: 287 us; the launch traced here: 286 us
  waiting for transfers between devices  109 us (38%)
  blocking collectives  67.8 us (24%)
  matrix products  33.3 us (12%)
  other arithmetic  25.9 us (9%)
  local copies, waits for them, and re-layouts  17.6 us (6%)
  starting transfers between devices  17.3 us (6%)
  between operations  15.2 us (5%)
    psum x1, waiting for transfers between devices, per_device(): lax.psum(mixer_part.astype(jnp.bfloat16), 'tp').astype(jnp.float32)  67.8 us
    reduce_scatter x1, waiting for transfers between devices, per_device(): lax.psum_scatter(ff_part.astype(jnp.bfloat16), 'tp', scatter_dimension=1,...  36.9 us
    all_gather x1, blocking collectives, per_device(): lax.all_gather(w_value_side, FS, axis=0, tiled=True)  21.1 us
    all_gather x1, blocking collectives, per_device(): lax.all_gather(w_gate_side, FS, axis=0, tiled=True)  18.7 us
    all_gather x1, blocking collectives, per_device(): lax.all_gather(w_mixer_out, FS, axis=1, tiled=True)  17.1 us
    all_to_all x2, starting transfers between devices, sent_to_all(): lax.all_to_all(jnp.broadcast_to(array[None], (devices, *array.shape)), ax...  17 us
    dot_general x3, matrix products, add_rows(): return jnp.dot(left, piece, preferred_element_type=jnp.float32)  16.2 us
    add x2, other arithmetic, causal_taps(): padded[:, 0:SEQ] * taps[0] + padded[:, 1:SEQ + 1] * taps[1]  12 us
  transfers between devices with their start and end apart: 6, of which 3 were waited for; matrix products, arithmetic and copies ran while one was open for 16% of the time, Pallas kernels for 0%

commit v1 on v0

v1 whole, which is shorter than its diff:
```python
import jax
import jax.numpy as jnp
from jax import lax
from jax.experimental import pallas as pl
from jax.experimental.pallas import tpu as pltpu
from jax.sharding import Mesh
from jax.sharding import PartitionSpec as P

ROWS = 1024
D = 2048
SG_WIDTH = 1024
SEQ = 256
FS = ("z", "y")
TP = ("x", "c")
SCALE = 2.0**0.25
EPS = 1e-05
F32 = jnp.float32
BF16 = jnp.bfloat16
MESH = pl.DeviceIdType.MESH


def mul(i, n):
    return pl.multiple_of(i, n)


def dot(a, b):
    return jnp.dot(a, b, preferred_element_type=F32)


ORDER = ((1, 0), (3, 0), (0, 1), (2, 0), (1, 3), (3, 3), (2, 1))
LAST = ((0, 3), (1, 1), (3, 1), (2, 3), (0, 2), (1, 2), (3, 2), (2, 2))


class PlaneGather:
    def __init__(self, block, pos, send_sem, recv_sem, flip=0):
        self.block, self.pos = block, pos
        self.send_sem, self.recv_sem = send_sem, recv_sem
        self.flip = flip

    def axes(self, half):
        return ("y", "z") if half == 0 else ("z", "y")

    def ref(self, half, d):
        a1, a2 = self.axes(half)
        at = {
            a1: lax.rem(self.pos[a1] + 4 - d[0], 4),
            a2: lax.rem(self.pos[a2] + 4 - d[1], 4),
        }
        return self.block(half, at["z"] * 4 + at["y"])

    def copy(self, half, target, source, axis, step):
        ref = self.ref(half, source)
        i = target[0] * 4 + target[1]
        return pltpu.make_async_remote_copy(
            src_ref=ref,
            dst_ref=ref,
            send_sem=self.send_sem.at[half, i],
            recv_sem=self.recv_sem.at[half, i],
            device_id={axis: lax.rem(self.pos[axis] + 4 + step, 4)},
            device_id_type=MESH,
        )

    def route(self, half, target):
        a1, a2 = self.axes(half)
        d1, d2 = target
        if d2 == 0:
            if d1 == 2:
                plus = (half + self.flip) % 2 == 0
                return ((1, 0), a1, 1) if plus else ((3, 0), a1, -1)
            return ((0, 0), a1, 1 if d1 == 1 else -1)
        if d2 == 2:
            return ((d1, 1), a2, 1) if d1 % 2 == 0 else ((d1, 3), a2, -1)
        return ((d1, 0), a2, 1 if d2 == 1 else -1)

    def send(self, half, target):
        source, axis, step = self.route(half, target)
        self.copy(half, target, source, axis, step).start()

    def after(self, half, source):
        for target in ((1, 0), (3, 0), (2, 0)):
            if self.route(half, target)[0] == source:
                self.send(half, target)
        for d1 in range(4):
            for d2 in (1, 3, 2):
                if self.route(half, (d1, d2))[0] == source:
                    self.send(half, (d1, d2))

    def own(self):
        for half in (0, 1):
            self.after(half, (0, 0))

    def arrived(self, half, d):
        i = d[0] * 4 + d[1]
        ref = self.ref(half, d)
        pltpu.make_async_remote_copy(
            src_ref=ref,
            dst_ref=ref,
            send_sem=self.send_sem.at[half, i],
            recv_sem=self.recv_sem.at[half, i],
            device_id={"y": lax.rem(self.pos["y"] + 1, 4)},
            device_id_type=MESH,
        ).wait_recv()

    def step(self, *which):
        for k in which:
            for half in (0, 1):
                self.arrived(half, ORDER[k])
                self.after(half, ORDER[k])

    def rest(self):
        for d in LAST:
            for half in (0, 1):
                self.arrived(half, d)

    def sent(self):
        for half in (0, 1):
            for d1 in range(4):
                for d2 in range(4):
                    if d1 or d2:
                        source, axis, step = self.route(half, (d1, d2))
                        self.copy(half, (d1, d2), source, axis, step).wait_send()


class RingGather:
    def __init__(self, block, x, send_sem, recv_sem):
        self.block, self.x = block, x
        self.send_sem, self.recv_sem = send_sem, recv_sem

    def copy(self, back, part, slot, step):
        ref = self.block(lax.rem(self.x + 4 - back, 4), part)
        return pltpu.make_async_remote_copy(
            src_ref=ref,
            dst_ref=ref,
            send_sem=self.send_sem.at[slot],
            recv_sem=self.recv_sem.at[slot],
            device_id={"x": lax.rem(self.x + 4 + step, 4)},
            device_id_type=MESH,
        )

    def sends(self):
        return ((0, 0, 0, 1), (0, 1, 1, -1), (0, 1, 2, 1), (0, 0, 3, -1), (1, 0, 4, 1), (3, 1, 5, -1))

    def own(self):
        for c in self.sends()[:4]:
            self.copy(*c).start()

    def forward(self):
        self.copy(1, 0, 0, 1).wait_recv()
        self.copy(*self.sends()[4]).start()
        self.copy(3, 1, 1, 1).wait_recv()
        self.copy(*self.sends()[5]).start()

    def rest(self):
        self.copy(1, 1, 2, 1).wait_recv()
        self.copy(3, 0, 3, 1).wait_recv()
        self.copy(2, 0, 4, 1).wait_recv()
        self.copy(2, 1, 5, 1).wait_recv()

    def sent(self):
        for c in self.sends():
            self.copy(*c).wait_send()


class Stats:
    def __init__(self, ref, x, c, send_sem, recv_sem):
        self.ref, self.x, self.c = ref, x, c
        self.send_sem, self.recv_sem = send_sem, recv_sem

    def copies(self):
        out = []
        for k in (4, 5, 2, 6, 3, 7, 1):
            dx, dc = k // 2, k % 2
            out.append(
                pltpu.make_async_remote_copy(
                    src_ref=self.ref.at[0],
                    dst_ref=self.ref.at[k],
                    send_sem=self.send_sem.at[k],
                    recv_sem=self.recv_sem.at[k],
                    device_id={"x": lax.rem(self.x + dx, 4), "c": lax.rem(self.c + dc, 2)},
                    device_id_type=MESH,
                )
            )
        return out

    def start(self):
        for c in self.copies():
            c.start()

    def total(self):
        for c in self.copies():
            c.wait_recv()
        total = self.ref[0]
        for k in range(1, 8):
            total = total + self.ref[k]
        return total

    def sent(self):
        for c in self.copies():
            c.wait_send()


def spread(row):
    return jnp.broadcast_to(row, (128, 128)).T


def kernel(
    tok_h, gv_h, mo_h, in1_h, in2_h, wd_h, gain, wsp, bias, g1, taps, g2,
    out,
    tok, gv, mo, in1, in2, wd, ga, va, st1, st2, tot, so,
    msend, mrecv, mown, fn, hid, dsend, drecv, xs, xr2, xr1, acc,
    lsem, psend, precv, rsend, rrecv, ssend, srecv, dss, drs, xss, xrs,
):
    z, y = lax.axis_index("z"), lax.axis_index("y")
    x, c = lax.axis_index("x"), lax.axis_index("c")
    pos = {"z": z, "y": y}
    f = z * 4 + y
    j = x * 2 + c
    sib = {"c": 1 - c}

    gv_block = lambda half, b: gv.at[pl.ds(mul(b * 128 + half * 64, 64), 64), :]
    in1_block = lambda half, b: in1.at[pl.ds(mul(b * 128 + half * 64, 64), 64), :]
    in2_block = lambda half, b: in2.at[pl.ds(mul(b * 128 + half * 64, 64), 64), :]
    mo_block = lambda half, b: mo.at[
        pl.ds(mul(x * 128 + half * 64, 64), 64), pl.ds(mul(b * 128, 128), 128)
    ]
    wd_block = lambda half, b: wd.at[pl.ds(half * 352, 352), pl.ds(mul(b * 128, 128), 128)]
    g_gv = PlaneGather(gv_block, pos, psend.at[0], precv.at[0], 0)
    g_mo = PlaneGather(mo_block, pos, psend.at[1], precv.at[1], 1)
    g_in1 = PlaneGather(in1_block, pos, psend.at[2], precv.at[2], 0)
    g_in2 = PlaneGather(in2_block, pos, psend.at[3], precv.at[3], 1)
    g_wd = PlaneGather(wd_block, pos, psend.at[4], precv.at[4], 0)
    r_mo = RingGather(
        lambda b, part: mo.at[pl.ds(mul(b * 128 + part * 64, 64), 64), :], x, rsend.at[0], rrecv.at[0]
    )
    r_so = RingGather(
        lambda b, part: so.at[pl.ds(part * 512, 512), pl.ds(mul(b * 128, 128), 128)],
        x, rsend.at[1], rrecv.at[1],
    )
    s1 = Stats(st1, x, c, ssend.at[0], srecv.at[0])
    s2 = Stats(st2, x, c, ssend.at[1], srecv.at[1])

    loads = [
        pltpu.make_async_copy(gv_h, gv.at[pl.ds(mul(f * 128, 128), 128), :], lsem.at[0]),
        pltpu.make_async_copy(
            mo_h, mo.at[pl.ds(mul(x * 128, 128), 128), pl.ds(mul(f * 128, 128), 128)], lsem.at[1]
        ),
        pltpu.make_async_copy(in1_h, in1.at[pl.ds(mul(f * 128, 128), 128), :], lsem.at[2]),
        pltpu.make_async_copy(in2_h, in2.at[pl.ds(mul(f * 128, 128), 128), :], lsem.at[3]),
        pltpu.make_async_copy(
            wd_h, wd.at[pl.ds(0, 704), pl.ds(mul(f * 128, 128), 128)], lsem.at[4]
        ),
        pltpu.make_async_copy(tok_h, tok, lsem.at[5]),
    ]
    for l in loads:
        l.start()

    barrier = pltpu.get_barrier_semaphore()
    peers = [{a: lax.rem(pos[a] + s, 4)} for a in ("y", "z") for s in (1, 3)]
    peers += [
        {"x": lax.rem(x + k // 2, 4), "c": lax.rem(c + k % 2, 2)} for k in range(1, 8)
    ]
    for p in peers:
        pl.semaphore_signal(barrier, inc=1, device_id=p, device_id_type=MESH)
    wd[704:768, :] = jnp.zeros((64, D), BF16)
    loads[0].wait()
    pl.semaphore_wait(barrier, len(peers))

    g_gv.own()
    loads[1].wait()
    g_mo.own()
    g_gv.step(0, 1)
    loads[2].wait()
    g_mo.step(0, 1)
    g_gv.step(2, 3)
    g_mo.step(2, 3)
    g_in1.own()
    g_gv.step(4, 5, 6)
    g_mo.step(4, 5, 6)
    g_gv.rest()
    loads[5].wait()

    @pl.loop(0, 4)
    def _(i):
        r = pl.ds(mul(i * 256, 256), 256)
        pre = dot(tok[r, :], gv[...])
        act = jax.nn.gelu(pre)
        ga[r, :] = act[:, :128]
        va[r, :] = act[:, 128:]
        for h in range(2):
            v = act[h * 128 : h * 128 + 128, 128:].T
            st1[0, pl.ds(i * 2 + h, 1), :] = jnp.sum(v, axis=0, keepdims=True)
            st1[0, pl.ds(i * 2 + h + 8, 1), :] = jnp.sum(v * v, axis=0, keepdims=True)

    s1.start()
    g_mo.rest()
    r_mo.own()
    g_in1.step(0, 1)
    loads[3].wait()
    g_in2.own()
    tot[...] = s1.total()

    lane = lax.broadcasted_iota(jnp.int32, (128, 128), 1)
    low = lax.broadcasted_iota(jnp.int32, (128, 128), 0) >= lane
    w0 = jnp.where(low, wsp[0], jnp.zeros((128, 128), BF16))
    w1 = jnp.where(low, wsp[1], jnp.zeros((128, 128), BF16))

    @pl.loop(0, 8)
    def _(n):
        r = pl.ds(mul(n * 128, 128), 128)
        mean = spread(tot[pl.ds(n, 1), :] * (1.0 / SG_WIDTH))
        square = spread(tot[pl.ds(n + 8, 1), :] * (1.0 / SG_WIDTH))
        inv = lax.rsqrt(square - mean * mean + EPS)
        vn = ((va[r, :] - mean) * inv * gain[...]).astype(BF16)
        mixed = jnp.where(lane < 64, dot(w0, vn), dot(w1, vn)) + bias[...]
        so[r, pl.ds(mul(x * 128, 128), 128)] = (ga[r, :] * mixed).astype(BF16)

    r_so.own()
    g_in1.step(2, 3)
    g_in1.step(4, 5, 6)
    loads[4].wait()
    g_in2.step(0, 1)
    r_mo.forward()
    r_so.forward()
    g_in2.step(2, 3)
    g_wd.own()
    g_in2.step(4, 5, 6)
    r_mo.rest()
    r_so.rest()

    theirs = (1 - c) * 512
    mine = c * 512

    def mix_copy(k):
        return pltpu.make_async_remote_copy(
            src_ref=msend.at[pl.ds(k * 256, 256), :],
            dst_ref=mrecv.at[pl.ds(k * 256, 256), :],
            send_sem=dss.at[k], recv_sem=drs.at[k], device_id=sib, device_id_type=MESH,
        )

    def fn_copy(k, base):
        ref = fn.at[pl.ds(mul(base + k * 256, 256), 256), :]
        return pltpu.make_async_remote_copy(
            src_ref=ref, dst_ref=ref,
            send_sem=dss.at[2 + k], recv_sem=drs.at[2 + k], device_id=sib, device_id_type=MESH,
        )

    for k in range(2):
        @pl.loop(0, 4)
        def _(i):
            cols = pl.ds(mul(i * 512, 512), 512)
            p = dot(so[pl.ds(mul(theirs + k * 256, 256), 256), :], mo[:, cols])
            msend[k * 256 : k * 256 + 256, cols] = p.astype(BF16)

        mix_copy(k).start()
    for k in range(2):
        @pl.loop(0, 4)
        def _(i):
            cols = pl.ds(mul(i * 512, 512), 512)
            mown[k * 256 : k * 256 + 256, cols] = dot(
                so[pl.ds(mul(mine + k * 256, 256), 256), :], mo[:, cols]
            )

    g_wd.step(0, 1)
    for k in range(2):
        mix_copy(k).wait_recv()

        @pl.loop(0, 8)
        def _(i):
            r = pl.ds(mul(k * 256 + i * 32, 32), 32)
            g = pl.ds(mul(mine + k * 256 + i * 32, 32), 32)
            v = SCALE * tok[g, :].astype(F32) + (mown[r, :] + mrecv[r, :].astype(F32))
            mean = jnp.sum(v, axis=1, keepdims=True) * (1.0 / D)
            square = jnp.sum(v * v, axis=1, keepdims=True) * (1.0 / D)
            inv = lax.rsqrt(square - mean * mean + EPS)
            fn[g, :] = ((v - mean) * inv * g1[...]).astype(BF16)

        fn_copy(k, mine).start()

    g_in1.rest()
    g_wd.step(2, 3)

    row = lax.broadcasted_iota(jnp.int32, (SEQ, 256), 0)
    lane2 = lax.broadcasted_iota(jnp.int32, (SEQ, 128), 1)

    def conv(p, t):
        n = p.shape[1]
        p1 = jnp.where(row[:, :n] >= 1, pltpu.roll(p, 1, 0), 0.0)
        p2 = jnp.where(row[:, :n] >= 2, pltpu.roll(p, 2, 0), 0.0)
        return p2 * t[0:1, :] + p1 * t[1:2, :] + p * t[2:3, :]

    def hidden(seq, buf, at, tile):
        r = pl.ds(mul(seq * SEQ, SEQ), SEQ)
        p = dot(fn[r, :], buf[:, pl.ds(mul(at * 256, 256), 256)])
        q = conv(p, taps[:, pl.ds(mul(tile * 256, 256), 256)])
        hid[r, pl.ds(mul(tile * 128, 128), 128)] = (
            jax.nn.silu(q[:, :128]) * q[:, 128:]
        ).astype(BF16)

    def hidden_last(seq):
        r = pl.ds(mul(seq * SEQ, SEQ), SEQ)
        p = dot(fn[r, :], in2[:, 512:640])
        q = conv(p, taps[:, 1280:1408])
        h = jax.nn.silu(q) * pltpu.roll(q, 64, 1)
        hid[r, 640:768] = jnp.where(lane2 < 64, h, 0.0).astype(BF16)

    own_seq = c * 2
    other_seq = (1 - c) * 2

    def part1(first):
        @pl.loop(0, 6)
        def _(i):
            hidden(first + i // 3, in1, i % 3, i % 3)

    def part2(first):
        @pl.loop(0, 4)
        def _(i):
            hidden(first + i // 2, in2, i % 2, 3 + i % 2)

        @pl.loop(0, 2)
        def _(i):
            hidden_last(first + i)

    part1(own_seq)
    g_wd.step(4, 5, 6)
    for k in range(2):
        fn_copy(k, (1 - c) * 512).wait_recv()
    part1(other_seq)
    g_in2.rest()
    part2(own_seq)
    part2(other_seq)
    g_wd.rest()

    hops = (2, 1, 3, 0)

    def dd_copy(k):
        cols = pl.ds(k * 256, 256)
        return pltpu.make_async_remote_copy(
            src_ref=dsend.at[:, cols], dst_ref=drecv.at[:, cols],
            send_sem=dss.at[4 + k], recv_sem=drs.at[4 + k], device_id=sib, device_id_type=MESH,
        )

    def wd_cols(k, parity):
        t = lax.rem(x + hops[k], 4)
        return pl.ds(mul((t * 2 + parity) * 256, 256), 256)

    def down_theirs(k):
        cols = wd_cols(k, 1 - c)

        @pl.loop(0, 4)
        def _(i):
            r = pl.ds(mul(i * 256, 256), 256)
            dsend[r, k * 256 : k * 256 + 256] = dot(hid[r, :], wd[:, cols]).astype(BF16)

        dd_copy(k).start()

    def down_mine(k, i):
        r = pl.ds(mul(i * 256, 256), 256)
        return dot(hid[r, :], wd[:, wd_cols(k, c)]) + drecv[r, k * 256 : k * 256 + 256].astype(F32)

    def x_copy(slot, src, dst, step):
        return pltpu.make_async_remote_copy(
            src_ref=src, dst_ref=dst, send_sem=xss.at[slot], recv_sem=xrs.at[slot],
            device_id={"x": lax.rem(x + 4 + step, 4)}, device_id_type=MESH,
        )

    up, lo = pl.ds(0, 512), pl.ds(512, 512)
    x_copies = (
        x_copy(0, xs.at[0, up], xr2.at[up], 1),
        x_copy(1, xs.at[0, lo], xr2.at[lo], -1),
        x_copy(2, xs.at[1, lo], xr1.at[0, lo], 1),
        x_copy(3, xs.at[2, up], xr1.at[1, up], -1),
        x_copy(4, xs.at[1, up], xr1.at[0, up], 1),
        x_copy(5, xs.at[2, lo], xr1.at[1, lo], -1),
    )

    def fill(k, first, extra):
        @pl.loop(first, first + 2)
        def _(i):
            r = pl.ds(mul(i * 256, 256), 256)
            v = down_mine(k, i)
            if extra:
                v = v + xr2[r, :].astype(F32)
            xs[k, r, :] = v.astype(BF16)

    down_theirs(0)
    down_theirs(1)
    dd_copy(0).wait_recv()
    fill(0, 0, False)
    x_copies[0].start()
    fill(0, 2, False)
    x_copies[1].start()
    down_theirs(2)
    dd_copy(1).wait_recv()
    fill(1, 2, False)
    x_copies[2].start()
    dd_copy(2).wait_recv()
    fill(2, 0, False)
    x_copies[3].start()
    down_theirs(3)
    x_copies[0].wait_recv()
    fill(1, 0, True)
    x_copies[4].start()
    x_copies[1].wait_recv()
    fill(2, 2, True)
    x_copies[5].start()
    dd_copy(3).wait_recv()

    @pl.loop(0, 4)
    def _(i):
        r = pl.ds(mul(i * 256, 256), 256)
        acc[r, :] = down_mine(3, i) + SCALE * fn[r, pl.ds(mul(j * 256, 256), 256)].astype(F32)

    for k in (2, 3, 4, 5):
        x_copies[k].wait_recv()

    @pl.loop(0, 8)
    def _(n):
        r = pl.ds(mul(n * 128, 128), 128)
        v = acc[r, :] + (xr1[0, r, :].astype(F32) + xr1[1, r, :].astype(F32))
        acc[r, :] = v
        a, b = v[:, :128], v[:, 128:]
        st2[0, pl.ds(n, 1), :] = jnp.sum((a + b).T, axis=0, keepdims=True)
        st2[0, pl.ds(n + 8, 1), :] = jnp.sum((a * a + b * b).T, axis=0, keepdims=True)

    s2.start()
    gain2 = g2[pl.ds(j, 1), :]
    for g in (g_gv, g_mo, g_in1, g_in2, g_wd, r_mo, r_so, s1):
        g.sent()
    for k in range(2):
        mix_copy(k).wait_send()
        fn_copy(k, mine).wait_send()
    for k in range(4):
        dd_copy(k).wait_send()
    for k in range(6):
        x_copies[k].wait_send()
    tot[...] = s2.total()

    @pl.loop(0, 8)
    def _(n):
        r = pl.ds(mul(n * 128, 128), 128)
        mean = spread(tot[pl.ds(n, 1), :] * (1.0 / D))
        square = spread(tot[pl.ds(n + 8, 1), :] * (1.0 / D))
        inv = lax.rsqrt(square - mean * mean + EPS)
        for h in range(2):
            cols = slice(h * 128, h * 128 + 128)
            out[r, cols] = ((acc[r, cols] - mean) * inv * gain2[:, cols]).astype(BF16)

    s2.sent()


def pairs(gate, up):
    tiles = []
    for i in range(5):
        tiles += [gate[:, i * 128 : i * 128 + 128], up[:, i * 128 : i * 128 + 128]]
    return tiles + [gate[:, 640:], up[:, 640:]]


def per_device(
    tokens, w_gate_side, w_value_side, spatial_gain, w_spatial, spatial_bias, w_mixer_out,
    first_gain, w_ff_gate, w_ff_up, conv_gate_taps, conv_up_taps, w_ff_down, second_gain,
):
    gv = jnp.concatenate([w_gate_side, w_value_side], axis=1)
    cut = pairs(w_ff_gate, w_ff_up)
    in1 = jnp.concatenate(cut[:6], axis=1)
    in2 = jnp.concatenate(cut[6:], axis=1)
    taps = jnp.concatenate(pairs(conv_gate_taps, conv_up_taps), axis=1)
    bias = jnp.repeat(spatial_bias.T, 64, axis=1)
    vmem = pl.BlockSpec(memory_space=pltpu.VMEM)
    hbm = pl.BlockSpec(memory_space=pl.ANY)
    V, DMA = pltpu.VMEM, pltpu.SemaphoreType.DMA
    return pl.pallas_call(
        kernel,
        out_shape=jax.ShapeDtypeStruct((ROWS, 256), BF16),
        in_specs=[hbm] * 6 + [vmem] * 6,
        out_specs=vmem,
        scratch_shapes=[
            V((ROWS, D), BF16),
            V((D, 256), BF16),
            V((512, D), BF16),
            V((D, 768), BF16),
            V((D, 640), BF16),
            V((768, D), BF16),
            V((ROWS, 128), F32),
            V((ROWS, 128), F32),
            V((8, 16, 128), F32),
            V((8, 16, 128), F32),
            V((16, 128), F32),
            V((ROWS, 512), BF16),
            V((512, D), BF16),
            V((512, D), BF16),
            V((512, D), F32),
            V((ROWS, D), BF16),
            V((ROWS, 768), BF16),
            V((ROWS, 1024), BF16),
            V((ROWS, 1024), BF16),
            V((3, ROWS, 256), BF16),
            V((ROWS, 256), BF16),
            V((2, ROWS, 256), BF16),
            V((ROWS, 256), F32),
            DMA((6,)),
            DMA((5, 2, 16)),
            DMA((5, 2, 16)),
            DMA((2, 6)),
            DMA((2, 6)),
            DMA((2, 8)),
            DMA((2, 8)),
            DMA((8,)),
            DMA((8,)),
            DMA((6,)),
            DMA((6,)),
        ],
        compiler_params=pltpu.CompilerParams(
            collective_id=0, has_side_effects=True, vmem_limit_bytes=60 * 1024 * 1024
        ),
    )(
        tokens, gv, w_mixer_out, in1, in2, w_ff_down, spatial_gain.reshape(1, 128), w_spatial,
        bias, first_gain.reshape(1, D), taps, second_gain.reshape(8, 256),
    )


def solution(mesh):
    finer = Mesh(mesh.devices.reshape(4, 4, 4, 2), ("z", "y", "x", "c"))
    in_specs = (
        P(FS, None), P(FS, TP), P(FS, TP), P(TP), P(TP, None, None), P(TP, None), P(TP, FS), P(),
        P(FS, TP), P(FS, TP), P(None, TP), P(None, TP), P(TP, FS), P(),
    )
    return jax.shard_map(
        per_device, mesh=finer, in_specs=in_specs, out_specs=P(FS, TP), check_vma=False
    )
```

time: 287 us -> 126 us (0.44)
  Pallas kernels: 0 us -> 111 us
  waiting for transfers between devices: 109 us -> 0 us
  blocking collectives: 67.8 us -> 0 us
  matrix products: 33.3 us -> 0 us
  other arithmetic: 25.9 us -> 1.39 us
  starting transfers between devices: 17.3 us -> 0 us
  between operations: 15.2 us -> 0.12 us
  local copies, waits for them, and re-layouts: 17.6 us -> 13.5 us
    pallas_call x0 -> x1, Pallas kernels: none -> 111 us  [per_device(): pl.pallas_call(kernel, out_shape=jax.ShapeDtypeStruct((ROWS, 256), BF16),...]
    all_gather x4 -> x0, blocking collectives: 67.8 us -> none  [the longest x1 21.1 us: per_device(): lax.all_gather(w_value_side, FS, axis=0, tiled=True)]
    psum x1 -> x0, waiting for transfers between devices: 67.8 us -> none  [per_device(): lax.psum(mixer_part.astype(jnp.bfloat16), 'tp').astype(jnp.float32)]
    reduce_scatter x1 -> x0, waiting for transfers between devices: 36.9 us -> none  [per_device(): lax.psum_scatter(ff_part.astype(jnp.bfloat16), 'tp', scatter_dimension=1,...]
    dot_general x6 -> x0, matrix products: 33.3 us -> none  [the longest x3 16.2 us: add_rows(): return jnp.dot(left, piece, preferred_element_type=jnp.float32)]
    all_to_all x2 -> x0, starting transfers between devices: 17 us -> none  [sent_to_all(): lax.all_to_all(jnp.broadcast_to(array[None], (devices, *array.shape)), ax...]
    add x2 -> x0, other arithmetic: 12 us -> none  [causal_taps(): padded[:, 0:SEQ] * taps[0] + padded[:, 1:SEQ + 1] * taps[1]]
    reduce_sum x4 -> x0, other arithmetic: 6.78 us -> none  [the longest x1 5.08 us: whole_norm(): mean = jnp.sum(values, axis=-1, keepdims=True) / width]
  transfers between devices with their start and end apart: 6 -> 0, of which waited for: 3 -> 0; matrix products, arithmetic and copies ran while one was open for 16% -> 0% of each run, Pallas kernels for 0% -> 0%
where the time goes in v1:
time: 126 us
  Pallas kernels  111 us (88%)
  local copies, waits for them, and re-layouts  13.5 us (11%)
  other arithmetic  1.39 us (1%)
    pallas_call x1, Pallas kernels, per_device(): pl.pallas_call(kernel, out_shape=jax.ShapeDtypeStruct((ROWS, 256), BF16),...  111 us
    unnamed x20, local copies, waits for them, and re-layouts  4.01 us
    slice x4, local copies, waits for them, and re-layouts, pairs(): return tiles + [gate[:, 640:], up[:, 640:]]  2.81 us

profile of v1, /device:TPU:1, one launch (start us, length us, event | category | flops | bytes accessed | tf_op | source)
XLA Modules:
  0.0 125.7 jit_solution(1901161197454369663)
XLA Ops:
  0.0 0.7 slice.94
  0.7 0.7 slice.95
  1.4 1.3 %reshape.15.g2 = f32[8,256]{1,0:T(8,128)} reshape(f32[2048]{0:T(1024)} %param.27) | data formatting | bytes 16384 | tf_op jit(solution)/shard_map/reshape | solution.py:617
  2.7 0.7 slice.82
  3.4 0.1 copy.51
  3.5 0.7 slice.83
  4.2 0.1 copy.52
  4.3 0.8 fusion.2
  5.2 0.7 concatenate.15.taps
  5.9 1.4 %pad_maximum_fusion.gv_h = bf16[128,256]{1,0:T(8,128)(2,1)} fusion(bf16[128,128]{1,0:T(8,128)(2,1)} %param.16, bf16[128,128]{1,0:T(8,128)(2,1)} %param.15), kind=kLoop, calls=%fused_computation | loop fusion | flops 131072 | bytes 131072 | tf_op jit(solution)/shard_map/concatenate | solution.py:562
  7.3 0.7 broadcast_in_dim.3
  7.9 0.7 copy.40.bias
  8.7 0.8 fusion.1
  9.5 0.1 copy.49
  9.6 0.1 copy.47
  9.7 0.1 copy.45
  9.9 0.1 copy.43
  10.0 0.1 copy.41
  10.1 0.8 fusion
  11.0 0.1 copy.50
  11.1 0.1 copy.48
  11.2 0.8 concatenate.14.in2_h
  12.0 0.1 copy.46
  12.1 0.1 copy.44
  12.2 0.1 copy.42
  12.4 0.0 copy-start
  12.4 0.7 copy-done
  13.1 110.7 %shard_map.136 = bf16[1024,256]{1,0:T(8,128)(2,1)} custom-call(bf16[1024,2048]{1,0:T(8,128)(2,1)} %tok_h.1, bf16[128,256]{1,0:T(8,128)(2,1)} %pad_maximum_fusion.gv_h, bf16[128,128]{1,0:T(8,128)(2,1)} %mo_h.1, bf16[128,768]{1,0:T(8,128)(2,1)} %copy-done, bf16[128,640]{1,0:T(8,128)(2,1)} %concatenate.14.in2_h, bf16[704,128]{1,0:T(8,128)(2,1)} %wd_h.1, ...), custom_call_target="tpu_custom_call" | custom-call | tf_op jit(solution)/shard_map/pallas_call | solution.py:571
  123.8 1.9 %copy.59 = bf16[1024,256]{1,0:T(8,128)(2,1)} copy(bf16[1024,256]{1,0:T(8,128)(2,1)} %shard_map.136) | data formatting | bytes 1048576
  (6 shorter events, 0.1 us)
Async XLA Ops:
  12.4 0.7 copy-start

commit v2 on v1

--- a/solution.py
+++ b/solution.py
@@ -32,8 +32,8 @@
 
 
 class PlaneGather:
-    def __init__(self, block, pos, send_sem, recv_sem, flip=0):
-        self.block, self.pos = block, pos
+    def __init__(self, block, pos, send_sem, recv_sem, flip=0, then=None):
+        self.block, self.pos, self.then = block, pos, then
         self.send_sem, self.recv_sem = send_sem, recv_sem
         self.flip = flip
 
@@ -76,18 +76,20 @@
         source, axis, step = self.route(half, target)
         self.copy(half, target, source, axis, step).start()
 
-    def after(self, half, source):
+    def after(self, half, source, first=True, second=True):
         for target in ((1, 0), (3, 0), (2, 0)):
-            if self.route(half, target)[0] == source:
+            if first and self.route(half, target)[0] == source:
                 self.send(half, target)
-        for d1 in range(4):
+        for d1 in range(4) if second else ():
             for d2 in (1, 3, 2):
                 if self.route(half, (d1, d2))[0] == source:
                     self.send(half, (d1, d2))
 
-    def own(self):
+    def own(self, first=True, second=True):
         for half in (0, 1):
-            self.after(half, (0, 0))
+            self.after(half, (0, 0), first, second)
+            if self.then:
+                self.then(half, self.ref(half, (0, 0)))
 
     def arrived(self, half, d):
         i = d[0] * 4 + d[1]
@@ -100,6 +102,8 @@
             device_id={"y": lax.rem(self.pos["y"] + 1, 4)},
             device_id_type=MESH,
         ).wait_recv()
+        if self.then:
+            self.then(half, ref)
 
     def step(self, *which):
         for k in which:
@@ -143,6 +147,17 @@
     def own(self):
         for c in self.sends()[:4]:
             self.copy(*c).start()
+
+    def piece(self, part, ref):
+        for slot, step in ((0, 1), (3, -1)) if part == 0 else ((2, 1), (1, -1)):
+            pltpu.make_async_remote_copy(
+                src_ref=ref,
+                dst_ref=ref,
+                send_sem=self.send_sem.at[slot],
+                recv_sem=self.recv_sem.at[slot],
+                device_id={"x": lax.rem(self.x + 4 + step, 4)},
+                device_id_type=MESH,
+            ).start()
 
     def forward(self):
         self.copy(1, 0, 0, 1).wait_recv()
@@ -204,11 +219,11 @@
 
 
 def kernel(
-    tok_h, gv_h, mo_h, in1_h, in2_h, wd_h, gain, wsp, bias, g1, taps, g2,
+    tok_h, gate_h, value_h, mo_h, fg_h, fu_h, wd_h, gain, wsp, bias, g1, taps_g, taps_u, g2,
     out,
-    tok, gv, mo, in1, in2, wd, ga, va, st1, st2, tot, so,
+    tok, wgt, wvl, mo, wfg, wfu, wd, ga, va, st1, st2, tot, so, taps,
     msend, mrecv, mown, fn, hid, dsend, drecv, xs, xr2, xr1, acc,
-    lsem, psend, precv, rsend, rrecv, ssend, srecv, dss, drs, xss, xrs,
+    lsem, psend, precv, rsend, rrecv, ssend, srecv, dss, drs, dds, ddr, xss, xrs,
 ):
     z, y = lax.axis_index("z"), lax.axis_index("y")
     x, c = lax.axis_index("x"), lax.axis_index("c")
@@ -217,39 +232,42 @@
     j = x * 2 + c
     sib = {"c": 1 - c}
 
-    gv_block = lambda half, b: gv.at[pl.ds(mul(b * 128 + half * 64, 64), 64), :]
-    in1_block = lambda half, b: in1.at[pl.ds(mul(b * 128 + half * 64, 64), 64), :]
-    in2_block = lambda half, b: in2.at[pl.ds(mul(b * 128 + half * 64, 64), 64), :]
-    mo_block = lambda half, b: mo.at[
-        pl.ds(mul(x * 128 + half * 64, 64), 64), pl.ds(mul(b * 128, 128), 128)
-    ]
-    wd_block = lambda half, b: wd.at[pl.ds(half * 352, 352), pl.ds(mul(b * 128, 128), 128)]
+    def gv_block(half, b):
+        return (wgt, wvl)[half].at[pl.ds(mul(b * 128, 128), 128), :]
+
+    def mo_block(half, b):
+        return mo.at[b, pl.ds(mul(x * 128 + half * 64, 64), 64), :]
+
+    def in1_block(half, b):
+        return (wfg, wfu)[half].at[b, pl.ds(0, 384), :]
+
+    def in2_block(half, b):
+        return (wfg, wfu)[half].at[b, pl.ds(384, 320), :]
+
+    def wd_block(half, b):
+        return wd.at[b, pl.ds(half * 352, 352), :]
+
+    r_mo = RingGather(
+        lambda b, part: mo.at[:, pl.ds(mul(b * 128 + part * 64, 64), 64), :], x, rsend.at[0], rrecv.at[0]
+    )
+    r_so = RingGather(lambda b, part: so.at[b, pl.ds(part * 512, 512), :], x, rsend.at[1], rrecv.at[1])
     g_gv = PlaneGather(gv_block, pos, psend.at[0], precv.at[0], 0)
-    g_mo = PlaneGather(mo_block, pos, psend.at[1], precv.at[1], 1)
+    g_mo = PlaneGather(mo_block, pos, psend.at[1], precv.at[1], 1, r_mo.piece)
     g_in1 = PlaneGather(in1_block, pos, psend.at[2], precv.at[2], 0)
     g_in2 = PlaneGather(in2_block, pos, psend.at[3], precv.at[3], 1)
     g_wd = PlaneGather(wd_block, pos, psend.at[4], precv.at[4], 0)
-    r_mo = RingGather(
-        lambda b, part: mo.at[pl.ds(mul(b * 128 + part * 64, 64), 64), :], x, rsend.at[0], rrecv.at[0]
-    )
-    r_so = RingGather(
-        lambda b, part: so.at[pl.ds(part * 512, 512), pl.ds(mul(b * 128, 128), 128)],
-        x, rsend.at[1], rrecv.at[1],
-    )
     s1 = Stats(st1, x, c, ssend.at[0], srecv.at[0])
     s2 = Stats(st2, x, c, ssend.at[1], srecv.at[1])
 
+    rows_f = pl.ds(mul(f * 128, 128), 128)
     loads = [
-        pltpu.make_async_copy(gv_h, gv.at[pl.ds(mul(f * 128, 128), 128), :], lsem.at[0]),
-        pltpu.make_async_copy(
-            mo_h, mo.at[pl.ds(mul(x * 128, 128), 128), pl.ds(mul(f * 128, 128), 128)], lsem.at[1]
-        ),
-        pltpu.make_async_copy(in1_h, in1.at[pl.ds(mul(f * 128, 128), 128), :], lsem.at[2]),
-        pltpu.make_async_copy(in2_h, in2.at[pl.ds(mul(f * 128, 128), 128), :], lsem.at[3]),
-        pltpu.make_async_copy(
-            wd_h, wd.at[pl.ds(0, 704), pl.ds(mul(f * 128, 128), 128)], lsem.at[4]
-        ),
-        pltpu.make_async_copy(tok_h, tok, lsem.at[5]),
+        pltpu.make_async_copy(gate_h, wgt.at[rows_f, :], lsem.at[0]),
+        pltpu.make_async_copy(value_h, wvl.at[rows_f, :], lsem.at[1]),
+        pltpu.make_async_copy(mo_h, mo.at[f, pl.ds(mul(x * 128, 128), 128), :], lsem.at[2]),
+        pltpu.make_async_copy(fg_h, wfg.at[f], lsem.at[3]),
+        pltpu.make_async_copy(fu_h, wfu.at[f], lsem.at[4]),
+        pltpu.make_async_copy(wd_h, wd.at[f, pl.ds(0, 704), :], lsem.at[5]),
+        pltpu.make_async_copy(tok_h, tok, lsem.at[6]),
     ]
     for l in loads:
         l.start()
@@ -261,28 +279,39 @@
     ]
     for p in peers:
         pl.semaphore_signal(barrier, inc=1, device_id=p, device_id_type=MESH)
-    wd[704:768, :] = jnp.zeros((64, D), BF16)
-    loads[0].wait()
+    for b in range(16):
+        wd[b, 704:768, :] = jnp.zeros((64, 128), BF16)
+    for i in range(5):
+        t = slice(i * 128, i * 128 + 128)
+        taps[0:3, i * 256 : i * 256 + 128] = taps_g[:, t]
+        taps[0:3, i * 256 + 128 : i * 256 + 256] = taps_u[:, t]
+    taps[0:3, 1280:1344] = taps_g[:, 640:704]
+    taps[0:3, 1344:1408] = taps_u[:, 640:704]
+    for k in range(3):
+        loads[k].wait()
     pl.semaphore_wait(barrier, len(peers))
 
+    g_mo.own()
     g_gv.own()
-    loads[1].wait()
-    g_mo.own()
+    g_mo.step(0, 1)
     g_gv.step(0, 1)
-    loads[2].wait()
-    g_mo.step(0, 1)
+    g_mo.step(2, 3)
     g_gv.step(2, 3)
-    g_mo.step(2, 3)
-    g_in1.own()
+    loads[3].wait()
+    loads[4].wait()
+    g_in1.own(second=False)
+    g_mo.step(4, 5, 6)
     g_gv.step(4, 5, 6)
-    g_mo.step(4, 5, 6)
+    g_in1.own(first=False)
+    g_mo.rest()
     g_gv.rest()
-    loads[5].wait()
+    loads[6].wait()
+    g_in1.step(0, 1)
 
     @pl.loop(0, 4)
     def _(i):
         r = pl.ds(mul(i * 256, 256), 256)
-        pre = dot(tok[r, :], gv[...])
+        pre = dot(tok[r, :], jnp.concatenate([wgt[...], wvl[...]], axis=1))
         act = jax.nn.gelu(pre)
         ga[r, :] = act[:, :128]
         va[r, :] = act[:, 128:]
@@ -292,17 +321,16 @@
             st1[0, pl.ds(i * 2 + h + 8, 1), :] = jnp.sum(v * v, axis=0, keepdims=True)
 
     s1.start()
-    g_mo.rest()
-    r_mo.own()
-    g_in1.step(0, 1)
-    loads[3].wait()
-    g_in2.own()
+    g_in1.step(2)
+    g_in2.own(second=False)
+    r_mo.forward()
     tot[...] = s1.total()
 
     lane = lax.broadcasted_iota(jnp.int32, (128, 128), 1)
     low = lax.broadcasted_iota(jnp.int32, (128, 128), 0) >= lane
     w0 = jnp.where(low, wsp[0], jnp.zeros((128, 128), BF16))
     w1 = jnp.where(low, wsp[1], jnp.zeros((128, 128), BF16))
+    shift = jnp.where(lane < 64, spread(bias[0:1, :]), spread(bias[1:2, :]))
 
     @pl.loop(0, 8)
     def _(n):
@@ -311,19 +339,18 @@
         square = spread(tot[pl.ds(n + 8, 1), :] * (1.0 / SG_WIDTH))
         inv = lax.rsqrt(square - mean * mean + EPS)
         vn = ((va[r, :] - mean) * inv * gain[...]).astype(BF16)
-        mixed = jnp.where(lane < 64, dot(w0, vn), dot(w1, vn)) + bias[...]
-        so[r, pl.ds(mul(x * 128, 128), 128)] = (ga[r, :] * mixed).astype(BF16)
+        mixed = jnp.where(lane < 64, dot(w0, vn), dot(w1, vn)) + shift
+        so[x, r, :] = (ga[r, :] * mixed).astype(BF16)
 
     r_so.own()
-    g_in1.step(2, 3)
+    g_in1.step(3)
+    g_in2.own(first=False)
     g_in1.step(4, 5, 6)
-    loads[4].wait()
     g_in2.step(0, 1)
-    r_mo.forward()
     r_so.forward()
     g_in2.step(2, 3)
+    loads[5].wait()
     g_wd.own()
-    g_in2.step(4, 5, 6)
     r_mo.rest()
     r_so.rest()
 
@@ -344,22 +371,25 @@
             send_sem=dss.at[2 + k], recv_sem=drs.at[2 + k], device_id=sib, device_id_type=MESH,
         )
 
+    def mix(base, i):
+        r = pl.ds(mul(base, 256), 256)
+        left = jnp.concatenate([so[b, r, :] for b in range(4)], axis=1)
+        return dot(left, jnp.concatenate([mo[i * 4 + q] for q in range(4)], axis=1))
+
     for k in range(2):
         @pl.loop(0, 4)
         def _(i):
-            cols = pl.ds(mul(i * 512, 512), 512)
-            p = dot(so[pl.ds(mul(theirs + k * 256, 256), 256), :], mo[:, cols])
-            msend[k * 256 : k * 256 + 256, cols] = p.astype(BF16)
+            msend[k * 256 : k * 256 + 256, pl.ds(mul(i * 512, 512), 512)] = mix(
+                theirs + k * 256, i
+            ).astype(BF16)
 
         mix_copy(k).start()
     for k in range(2):
         @pl.loop(0, 4)
         def _(i):
-            cols = pl.ds(mul(i * 512, 512), 512)
-            mown[k * 256 : k * 256 + 256, cols] = dot(
-                so[pl.ds(mul(mine + k * 256, 256), 256), :], mo[:, cols]
-            )
-
+            mown[k * 256 : k * 256 + 256, pl.ds(mul(i * 512, 512), 512)] = mix(mine + k * 256, i)
+
+    g_in2.step(4, 5, 6)
     g_wd.step(0, 1)
     for k in range(2):
         mix_copy(k).wait_recv()
@@ -388,9 +418,16 @@
         p2 = jnp.where(row[:, :n] >= 2, pltpu.roll(p, 2, 0), 0.0)
         return p2 * t[0:1, :] + p1 * t[1:2, :] + p * t[2:3, :]
 
-    def hidden(seq, buf, at, tile):
+    def dot_t(a, rows):
+        w = jnp.concatenate(
+            [jnp.concatenate([buf[b, rows, :] for b in range(16)], axis=1) for buf in (wfg, wfu)],
+            axis=0,
+        )
+        return lax.dot_general(a, w, (((1,), (1,)), ((), ())), preferred_element_type=F32)
+
+    def hidden(seq, tile):
         r = pl.ds(mul(seq * SEQ, SEQ), SEQ)
-        p = dot(fn[r, :], buf[:, pl.ds(mul(at * 256, 256), 256)])
+        p = dot_t(fn[r, :], pl.ds(mul(tile * 128, 128), 128))
         q = conv(p, taps[:, pl.ds(mul(tile * 256, 256), 256)])
         hid[r, pl.ds(mul(tile * 128, 128), 128)] = (
             jax.nn.silu(q[:, :128]) * q[:, 128:]
@@ -398,7 +435,7 @@
 
     def hidden_last(seq):
         r = pl.ds(mul(seq * SEQ, SEQ), SEQ)
-        p = dot(fn[r, :], in2[:, 512:640])
+        p = dot_t(fn[r, :], pl.ds(640, 64))
         q = conv(p, taps[:, 1280:1408])
         h = jax.nn.silu(q) * pltpu.roll(q, 64, 1)
         hid[r, 640:768] = jnp.where(lane2 < 64, h, 0.0).astype(BF16)
@@ -409,12 +446,12 @@
     def part1(first):
         @pl.loop(0, 6)
         def _(i):
-            hidden(first + i // 3, in1, i % 3, i % 3)
+            hidden(first + i // 3, i % 3)
 
     def part2(first):
         @pl.loop(0, 4)
         def _(i):
-            hidden(first + i // 2, in2, i % 2, 3 + i % 2)
+            hidden(first + i // 2, 3 + i % 2)
 
         @pl.loop(0, 2)
         def _(i):
@@ -432,30 +469,25 @@
 
     hops = (2, 1, 3, 0)
 
-    def dd_copy(k):
-        cols = pl.ds(k * 256, 256)
+    def dd_copy(k, h):
+        r = pl.ds(h * 512, 512)
         return pltpu.make_async_remote_copy(
-            src_ref=dsend.at[:, cols], dst_ref=drecv.at[:, cols],
-            send_sem=dss.at[4 + k], recv_sem=drs.at[4 + k], device_id=sib, device_id_type=MESH,
-        )
-
-    def wd_cols(k, parity):
-        t = lax.rem(x + hops[k], 4)
-        return pl.ds(mul((t * 2 + parity) * 256, 256), 256)
-
-    def down_theirs(k):
-        cols = wd_cols(k, 1 - c)
-
-        @pl.loop(0, 4)
-        def _(i):
-            r = pl.ds(mul(i * 256, 256), 256)
-            dsend[r, k * 256 : k * 256 + 256] = dot(hid[r, :], wd[:, cols]).astype(BF16)
-
-        dd_copy(k).start()
-
-    def down_mine(k, i):
-        r = pl.ds(mul(i * 256, 256), 256)
-        return dot(hid[r, :], wd[:, wd_cols(k, c)]) + drecv[r, k * 256 : k * 256 + 256].astype(F32)
+            src_ref=dsend.at[k, r, :], dst_ref=drecv.at[k, r, :],
+            send_sem=dds.at[k, h], recv_sem=ddr.at[k, h], device_id=sib, device_id_type=MESH,
+        )
+
+    def down(k, i, parity):
+        b = (lax.rem(x + hops[k], 4) * 2 + parity) * 2
+        return dot(
+            hid[pl.ds(mul(i * 256, 256), 256), :], jnp.concatenate([wd[b], wd[b + 1]], axis=1)
+        )
+
+    def down_theirs(k, h):
+        @pl.loop(h * 2, h * 2 + 2)
+        def _(i):
+            dsend[k, pl.ds(mul(i * 256, 256), 256), :] = down(k, i, 1 - c).astype(BF16)
+
+        dd_copy(k, h).start()
 
     def x_copy(slot, src, dst, step):
         return pltpu.make_async_remote_copy(
@@ -473,43 +505,55 @@
         x_copy(5, xs.at[2, lo], xr1.at[1, lo], -1),
     )
 
-    def fill(k, first, extra):
-        @pl.loop(first, first + 2)
+    def fill(k, h, slot, extra=False):
+        dd_copy(k, h).wait_recv()
+
+        @pl.loop(h * 2, h * 2 + 2)
         def _(i):
             r = pl.ds(mul(i * 256, 256), 256)
-            v = down_mine(k, i)
+            v = down(k, i, c) + drecv[k, r, :].astype(F32)
             if extra:
                 v = v + xr2[r, :].astype(F32)
             xs[k, r, :] = v.astype(BF16)
 
-    down_theirs(0)
-    down_theirs(1)
-    dd_copy(0).wait_recv()
-    fill(0, 0, False)
-    x_copies[0].start()
-    fill(0, 2, False)
-    x_copies[1].start()
-    down_theirs(2)
-    dd_copy(1).wait_recv()
-    fill(1, 2, False)
-    x_copies[2].start()
-    dd_copy(2).wait_recv()
-    fill(2, 0, False)
-    x_copies[3].start()
-    down_theirs(3)
+        x_copies[slot].start()
+
+    down_theirs(0, 0)
+    down_theirs(0, 1)
+    down_theirs(1, 1)
+    fill(0, 0, 0)
+    fill(0, 1, 1)
+    down_theirs(2, 0)
+    fill(1, 1, 2)
+    fill(2, 0, 3)
+    down_theirs(1, 0)
+    down_theirs(2, 1)
+    down_theirs(3, 0)
+    down_theirs(3, 1)
     x_copies[0].wait_recv()
-    fill(1, 0, True)
-    x_copies[4].start()
+    fill(1, 0, 4, True)
     x_copies[1].wait_recv()
-    fill(2, 2, True)
-    x_copies[5].start()
-    dd_copy(3).wait_recv()
-
-    @pl.loop(0, 4)
-    def _(i):
-        r = pl.ds(mul(i * 256, 256), 256)
-        acc[r, :] = down_mine(3, i) + SCALE * fn[r, pl.ds(mul(j * 256, 256), 256)].astype(F32)
-
+    fill(2, 1, 5, True)
+    for h in range(2):
+        dd_copy(3, h).wait_recv()
+
+        @pl.loop(h * 2, h * 2 + 2)
+        def _(i):
+            r = pl.ds(mul(i * 256, 256), 256)
+            acc[r, :] = (
+                down(3, i, c)
+                + drecv[3, r, :].astype(F32)
+                + SCALE * fn[r, pl.ds(mul(j * 256, 256), 256)].astype(F32)
+            )
+
+    for g in (g_gv, g_mo, g_in1, g_in2, g_wd, r_mo, r_so, s1):
+        g.sent()
+    for k in range(2):
+        mix_copy(k).wait_send()
+        fn_copy(k, mine).wait_send()
+    for k in range(4):
+        for h in range(2):
+            dd_copy(k, h).wait_send()
     for k in (2, 3, 4, 5):
         x_copies[k].wait_recv()
 
@@ -523,14 +567,7 @@
         st2[0, pl.ds(n + 8, 1), :] = jnp.sum((a * a + b * b).T, axis=0, keepdims=True)
 
     s2.start()
-    gain2 = g2[pl.ds(j, 1), :]
-    for g in (g_gv, g_mo, g_in1, g_in2, g_wd, r_mo, r_so, s1):
-        g.sent()
-    for k in range(2):
-        mix_copy(k).wait_send()
-        fn_copy(k, mine).wait_send()
-    for k in range(4):
-        dd_copy(k).wait_send()
+    gain2 = g2[:, pl.ds(mul(j * 256, 256), 256)]
     for k in range(6):
         x_copies[k].wait_send()
     tot[...] = s2.total()
@@ -548,64 +585,55 @@
     s2.sent()
 
 
-def pairs(gate, up):
-    tiles = []
-    for i in range(5):
-        tiles += [gate[:, i * 128 : i * 128 + 128], up[:, i * 128 : i * 128 + 128]]
-    return tiles + [gate[:, 640:], up[:, 640:]]
-
-
 def per_device(
     tokens, w_gate_side, w_value_side, spatial_gain, w_spatial, spatial_bias, w_mixer_out,
     first_gain, w_ff_gate, w_ff_up, conv_gate_taps, conv_up_taps, w_ff_down, second_gain,
 ):
-    gv = jnp.concatenate([w_gate_side, w_value_side], axis=1)
-    cut = pairs(w_ff_gate, w_ff_up)
-    in1 = jnp.concatenate(cut[:6], axis=1)
-    in2 = jnp.concatenate(cut[6:], axis=1)
-    taps = jnp.concatenate(pairs(conv_gate_taps, conv_up_taps), axis=1)
-    bias = jnp.repeat(spatial_bias.T, 64, axis=1)
     vmem = pl.BlockSpec(memory_space=pltpu.VMEM)
     hbm = pl.BlockSpec(memory_space=pl.ANY)
     V, DMA = pltpu.VMEM, pltpu.SemaphoreType.DMA
     return pl.pallas_call(
         kernel,
         out_shape=jax.ShapeDtypeStruct((ROWS, 256), BF16),
-        in_specs=[hbm] * 6 + [vmem] * 6,
+        in_specs=[hbm] * 7 + [vmem] * 7,
         out_specs=vmem,
         scratch_shapes=[
             V((ROWS, D), BF16),
-            V((D, 256), BF16),
-            V((512, D), BF16),
-            V((D, 768), BF16),
-            V((D, 640), BF16),
-            V((768, D), BF16),
+            V((D, 128), BF16),
+            V((D, 128), BF16),
+            V((16, 512, 128), BF16),
+            V((16, 704, 128), BF16),
+            V((16, 704, 128), BF16),
+            V((16, 768, 128), BF16),
             V((ROWS, 128), F32),
             V((ROWS, 128), F32),
             V((8, 16, 128), F32),
             V((8, 16, 128), F32),
             V((16, 128), F32),
-            V((ROWS, 512), BF16),
+            V((4, ROWS, 128), BF16),
+            V((8, 1408), F32),
             V((512, D), BF16),
             V((512, D), BF16),
             V((512, D), F32),
             V((ROWS, D), BF16),
             V((ROWS, 768), BF16),
-            V((ROWS, 1024), BF16),
-            V((ROWS, 1024), BF16),
+            V((4, ROWS, 256), BF16),
+            V((4, ROWS, 256), BF16),
             V((3, ROWS, 256), BF16),
             V((ROWS, 256), BF16),
             V((2, ROWS, 256), BF16),
             V((ROWS, 256), F32),
-            DMA((6,)),
+            DMA((7,)),
             DMA((5, 2, 16)),
             DMA((5, 2, 16)),
             DMA((2, 6)),
             DMA((2, 6)),
             DMA((2, 8)),
             DMA((2, 8)),
-            DMA((8,)),
-            DMA((8,)),
+            DMA((4,)),
+            DMA((4,)),
+            DMA((4, 2)),
+            DMA((4, 2)),
             DMA((6,)),
             DMA((6,)),
         ],
@@ -613,8 +641,9 @@
             collective_id=0, has_side_effects=True, vmem_limit_bytes=60 * 1024 * 1024
         ),
     )(
-        tokens, gv, w_mixer_out, in1, in2, w_ff_down, spatial_gain.reshape(1, 128), w_spatial,
-        bias, first_gain.reshape(1, D), taps, second_gain.reshape(8, 256),
+        tokens, w_gate_side, w_value_side, w_mixer_out, w_ff_gate.T, w_ff_up.T, w_ff_down,
+        spatial_gain.reshape(1, 128), w_spatial, spatial_bias, first_gain.reshape(1, D),
+        conv_gate_taps, conv_up_taps, second_gain.reshape(1, D),
     )
 
 

time: 126 us -> 111 us (0.88)
  local copies, waits for them, and re-layouts: 13.5 us -> 1.87 us
  Pallas kernels: 111 us -> 109 us
  other arithmetic: 1.39 us -> 0 us
    slice x7 -> x0, local copies, waits for them, and re-layouts: 5.32 us -> none  [the longest x4 2.81 us: pairs(): return tiles + [gate[:, 640:], up[:, 640:]]]
    unnamed x20 -> x1, local copies, waits for them, and re-layouts: 4.01 us -> 1.87 us
    reshape x2 -> x0, local copies, waits for them, and re-layouts: 2 us -> none  [the longest x1 1.29 us: per_device(): second_gain.reshape(8, 256)]
    pallas_call x1, Pallas kernels: 111 us -> 109 us  [per_device(): pl.pallas_call(kernel, out_shape=jax.ShapeDtypeStruct((ROWS, 256), BF16),...]
    concatenate x3 -> x0, local copies, waits for them, and re-layouts: 1.46 us -> none  [the longest x1 0.76 us: per_device(): in2 = jnp.concatenate(cut[6:], axis=1)]
    concatenate x1 -> x0, other arithmetic: 1.39 us -> none  [per_device(): gv = jnp.concatenate([w_gate_side, w_value_side], axis=1)]
where the time goes in v2:
time: 111 us
  Pallas kernels  109 us (98%)
  local copies, waits for them, and re-layouts  1.87 us (2%)
    pallas_call x1, Pallas kernels, per_device(): pl.pallas_call(kernel, out_shape=jax.ShapeDtypeStruct((ROWS, 256), BF16),...  109 us

profile of v2, /device:TPU:1, one launch (start us, length us, event | category | flops | bytes accessed | tf_op | source)
XLA Modules:
  0.0 111.0 jit_solution(13712034859078258181)
XLA Ops:
  0.0 109.2 %shard_map.136 = bf16[1024,256]{1,0:T(8,128)(2,1)} custom-call(bf16[1024,2048]{1,0:T(8,128)(2,1)} %tok_h.1, bf16[128,128]{1,0:T(8,128)(2,1)} %gate_h.1, bf16[128,128]{1,0:T(8,128)(2,1)} %value_h.1, bf16[128,128]{1,0:T(8,128)(2,1)} %mo_h.1, bf16[704,128]{1,0:T(8,128)(2,1)} %bitcast.5, bf16[704,128]{1,0:T(8,128)(2,1)} %bitcast.6, bf16[704,128]{1,0:T(8,128)(2,1)} %wd_h.1, ...), custom_call_target="tpu_custom_call" | custom-call | tf_op jit(solution)/shard_map/pallas_call | solution.py:595
  109.2 1.9 %copy.16 = bf16[1024,256]{1,0:T(8,128)(2,1)} copy(bf16[1024,256]{1,0:T(8,128)(2,1)} %shard_map.136) | data formatting | bytes 1048576

commit v3 on v2

--- a/solution.py
+++ b/solution.py
@@ -32,8 +32,8 @@
 
 
 class PlaneGather:
-    def __init__(self, block, pos, send_sem, recv_sem, flip=0, then=None):
-        self.block, self.pos, self.then = block, pos, then
+    def __init__(self, block, pos, send_sem, recv_sem, flip=0, then=None, direct=False):
+        self.block, self.pos, self.then, self.direct = block, pos, then, direct
         self.send_sem, self.recv_sem = send_sem, recv_sem
         self.flip = flip
 
@@ -63,6 +63,8 @@
     def route(self, half, target):
         a1, a2 = self.axes(half)
         d1, d2 = target
+        if self.direct:
+            return ((d1, 0), a2, d2) if d2 else ((0, 0), a1, d1)
         if d2 == 0:
             if d1 == 2:
                 plus = (half + self.flip) % 2 == 0
@@ -88,7 +90,7 @@
     def own(self, first=True, second=True):
         for half in (0, 1):
             self.after(half, (0, 0), first, second)
-            if self.then:
+            if self.then and first:
                 self.then(half, self.ref(half, (0, 0)))
 
     def arrived(self, half, d):
@@ -112,7 +114,7 @@
                 self.after(half, ORDER[k])
 
     def rest(self):
-        for d in LAST:
+        for d in LAST + (tuple(ORDER[k] for k in (2, 4, 5, 6)) if self.direct else ()):
             for half in (0, 1):
                 self.arrived(half, d)
 
@@ -126,12 +128,11 @@
 
 
 class RingGather:
-    def __init__(self, block, x, send_sem, recv_sem):
-        self.block, self.x = block, x
+    def __init__(self, block, x, send_sem, recv_sem, chunks):
+        self.block, self.x, self.chunks = block, x, chunks
         self.send_sem, self.recv_sem = send_sem, recv_sem
 
-    def copy(self, back, part, slot, step):
-        ref = self.block(lax.rem(self.x + 4 - back, 4), part)
+    def move(self, ref, slot, step):
         return pltpu.make_async_remote_copy(
             src_ref=ref,
             dst_ref=ref,
@@ -141,39 +142,49 @@
             device_id_type=MESH,
         )
 
+    def copy(self, back, part, slot, step):
+        return self.move(self.block(lax.rem(self.x + 4 - back, 4), part), slot, step)
+
+    def far_copy(self, back, part, chunk, step):
+        b = lax.rem(self.x + 4 - back, 4)
+        slot = 4 + part * self.chunks + chunk
+        return self.move(self.block(b, part, chunk), slot, step)
+
     def sends(self):
-        return ((0, 0, 0, 1), (0, 1, 1, -1), (0, 1, 2, 1), (0, 0, 3, -1), (1, 0, 4, 1), (3, 1, 5, -1))
-
-    def own(self):
-        for c in self.sends()[:4]:
-            self.copy(*c).start()
+        return ((0, 0, 0, 1), (0, 1, 1, -1), (0, 1, 2, 1), (0, 0, 3, -1))
+
+    def own(self, part):
+        for c in self.sends():
+            if c[1] == part:
+                self.copy(*c).start()
 
     def piece(self, part, ref):
         for slot, step in ((0, 1), (3, -1)) if part == 0 else ((2, 1), (1, -1)):
-            pltpu.make_async_remote_copy(
-                src_ref=ref,
-                dst_ref=ref,
-                send_sem=self.send_sem.at[slot],
-                recv_sem=self.recv_sem.at[slot],
-                device_id={"x": lax.rem(self.x + 4 + step, 4)},
-                device_id_type=MESH,
-            ).start()
-
-    def forward(self):
-        self.copy(1, 0, 0, 1).wait_recv()
-        self.copy(*self.sends()[4]).start()
-        self.copy(3, 1, 1, 1).wait_recv()
-        self.copy(*self.sends()[5]).start()
-
-    def rest(self):
+            self.move(ref, slot, step).start()
+
+    def forward(self, chunk):
+        if chunk == 0:
+            self.copy(1, 0, 0, 1).wait_recv()
+        self.far_copy(1, 0, chunk, 1).start()
+        if chunk == 0:
+            self.copy(3, 1, 1, 1).wait_recv()
+        self.far_copy(3, 1, chunk, -1).start()
+
+    def near(self):
         self.copy(1, 1, 2, 1).wait_recv()
         self.copy(3, 0, 3, 1).wait_recv()
-        self.copy(2, 0, 4, 1).wait_recv()
-        self.copy(2, 1, 5, 1).wait_recv()
+
+    def far(self):
+        for chunk in range(self.chunks):
+            for part in (0, 1):
+                self.far_copy(2, part, chunk, 1).wait_recv()
 
     def sent(self):
         for c in self.sends():
             self.copy(*c).wait_send()
+        for chunk in range(self.chunks):
+            self.far_copy(1, 0, chunk, 1).wait_send()
+            self.far_copy(3, 1, chunk, -1).wait_send()
 
 
 class Stats:
@@ -219,10 +230,10 @@
 
 
 def kernel(
-    tok_h, gate_h, value_h, mo_h, fg_h, fu_h, wd_h, gain, wsp, bias, g1, taps_g, taps_u, g2,
+    tok_h, gate_h, value_h, mo_h, fg_h, fu_h, wd_h, gain_h, wsp_h, bias_h, g1_h, tg_h, tu_h, g2_h,
     out,
-    tok, wgt, wvl, mo, wfg, wfu, wd, ga, va, st1, st2, tot, so, taps,
-    msend, mrecv, mown, fn, hid, dsend, drecv, xs, xr2, xr1, acc,
+    tok, wgt, wvl, mo, wfg, wfu, wd, ga, va, st1, st2, tot, so, taps, gain, wsp, bias, g1, taps_g, taps_u, g2,
+    msend, mrecv, mown, mtheir, fn, hid, dsend, drecv, xs, xr2, xr1, acc,
     lsem, psend, precv, rsend, rrecv, ssend, srecv, dss, drs, dds, ddr, xss, xrs,
 ):
     z, y = lax.axis_index("z"), lax.axis_index("y")
@@ -247,10 +258,15 @@
     def wd_block(half, b):
         return wd.at[b, pl.ds(half * 352, 352), :]
 
-    r_mo = RingGather(
-        lambda b, part: mo.at[:, pl.ds(mul(b * 128 + part * 64, 64), 64), :], x, rsend.at[0], rrecv.at[0]
-    )
-    r_so = RingGather(lambda b, part: so.at[b, pl.ds(part * 512, 512), :], x, rsend.at[1], rrecv.at[1])
+    def mo_ring(b, part, chunk=None):
+        cut = slice(None) if chunk is None else pl.ds(chunk * 8, 8)
+        return mo.at[cut, pl.ds(mul(b * 128 + part * 64, 64), 64), :]
+
+    def so_ring(b, part, chunk=None):
+        return so.at[b, pl.ds(part * 512, 512), :]
+
+    r_mo = RingGather(mo_ring, x, rsend.at[0], rrecv.at[0], 2)
+    r_so = RingGather(so_ring, x, rsend.at[1], rrecv.at[1], 1)
     g_gv = PlaneGather(gv_block, pos, psend.at[0], precv.at[0], 0)
     g_mo = PlaneGather(mo_block, pos, psend.at[1], precv.at[1], 1, r_mo.piece)
     g_in1 = PlaneGather(in1_block, pos, psend.at[2], precv.at[2], 0)
@@ -269,7 +285,16 @@
         pltpu.make_async_copy(wd_h, wd.at[f, pl.ds(0, 704), :], lsem.at[5]),
         pltpu.make_async_copy(tok_h, tok, lsem.at[6]),
     ]
-    for l in loads:
+    small = [
+        pltpu.make_async_copy(a, b, lsem.at[7 + k])
+        for k, (a, b) in enumerate(
+            zip(
+                (tg_h, tu_h, gain_h, wsp_h, bias_h, g1_h, g2_h),
+                (taps_g, taps_u, gain, wsp, bias, g1, g2),
+            )
+        )
+    ]
+    for l in loads + small:
         l.start()
 
     barrier = pltpu.get_barrier_semaphore()
@@ -281,6 +306,8 @@
         pl.semaphore_signal(barrier, inc=1, device_id=p, device_id_type=MESH)
     for b in range(16):
         wd[b, 704:768, :] = jnp.zeros((64, 128), BF16)
+    for l in small:
+        l.wait()
     for i in range(5):
         t = slice(i * 128, i * 128 + 128)
         taps[0:3, i * 256 : i * 256 + 128] = taps_g[:, t]
@@ -291,23 +318,36 @@
         loads[k].wait()
     pl.semaphore_wait(barrier, len(peers))
 
-    g_mo.own()
-    g_gv.own()
-    g_mo.step(0, 1)
-    g_gv.step(0, 1)
-    g_mo.step(2, 3)
-    g_gv.step(2, 3)
+    g_mo.own(second=False)
+    g_gv.own(second=False)
     loads[3].wait()
     loads[4].wait()
     g_in1.own(second=False)
-    g_mo.step(4, 5, 6)
-    g_gv.step(4, 5, 6)
+    g_gv.own(first=False)
+    g_mo.step(0)
+    g_mo.step(1)
+    g_gv.step(1)
+    g_gv.step(0)
+    g_mo.own(first=False)
+    g_in1.step(1)
+    g_gv.step(5)
+    g_mo.step(3)
+    g_mo.step(5)
+    g_gv.step(3)
+    g_gv.step(4)
+    g_mo.step(2)
+    g_mo.step(4)
+    g_in2.own(second=False)
+    g_gv.step(2)
+    g_mo.step(6)
+    g_gv.step(6)
+    g_in1.step(0)
+    loads[5].wait()
+    g_wd.own(second=False)
+    g_mo.rest()
     g_in1.own(first=False)
-    g_mo.rest()
     g_gv.rest()
     loads[6].wait()
-    g_in1.step(0, 1)
-
     @pl.loop(0, 4)
     def _(i):
         r = pl.ds(mul(i * 256, 256), 256)
@@ -321,39 +361,41 @@
             st1[0, pl.ds(i * 2 + h + 8, 1), :] = jnp.sum(v * v, axis=0, keepdims=True)
 
     s1.start()
-    g_in1.step(2)
-    g_in2.own(second=False)
-    r_mo.forward()
+    g_in2.step(0)
+    r_mo.forward(0)
+    g_in2.step(1)
+    g_wd.step(0)
     tot[...] = s1.total()
-
     lane = lax.broadcasted_iota(jnp.int32, (128, 128), 1)
     low = lax.broadcasted_iota(jnp.int32, (128, 128), 0) >= lane
     w0 = jnp.where(low, wsp[0], jnp.zeros((128, 128), BF16))
     w1 = jnp.where(low, wsp[1], jnp.zeros((128, 128), BF16))
     shift = jnp.where(lane < 64, spread(bias[0:1, :]), spread(bias[1:2, :]))
 
-    @pl.loop(0, 8)
-    def _(n):
-        r = pl.ds(mul(n * 128, 128), 128)
-        mean = spread(tot[pl.ds(n, 1), :] * (1.0 / SG_WIDTH))
-        square = spread(tot[pl.ds(n + 8, 1), :] * (1.0 / SG_WIDTH))
-        inv = lax.rsqrt(square - mean * mean + EPS)
-        vn = ((va[r, :] - mean) * inv * gain[...]).astype(BF16)
-        mixed = jnp.where(lane < 64, dot(w0, vn), dot(w1, vn)) + shift
-        so[x, r, :] = (ga[r, :] * mixed).astype(BF16)
-
-    r_so.own()
+    for part in range(2):
+        @pl.loop(part * 4, part * 4 + 4)
+        def _(n):
+            r = pl.ds(mul(n * 128, 128), 128)
+            mean = spread(tot[pl.ds(n, 1), :] * (1.0 / SG_WIDTH))
+            square = spread(tot[pl.ds(n + 8, 1), :] * (1.0 / SG_WIDTH))
+            inv = lax.rsqrt(square - mean * mean + EPS)
+            vn = ((va[r, :] - mean) * inv * gain[...]).astype(BF16)
+            mixed = jnp.where(lane < 64, dot(w0, vn), dot(w1, vn)) + shift
+            so[x, r, :] = (ga[r, :] * mixed).astype(BF16)
+
+        r_so.own(part)
+
+    g_wd.step(1)
+    r_mo.forward(1)
     g_in1.step(3)
+    g_in2.step(3)
     g_in2.own(first=False)
-    g_in1.step(4, 5, 6)
-    g_in2.step(0, 1)
-    r_so.forward()
-    g_in2.step(2, 3)
-    loads[5].wait()
-    g_wd.own()
-    r_mo.rest()
-    r_so.rest()
-
+    g_in1.step(2)
+    g_in1.step(4)
+    r_so.forward(0)
+    r_mo.near()
+    r_so.near()
+    g_in1.step(5)
     theirs = (1 - c) * 512
     mine = c * 512
 
@@ -371,26 +413,52 @@
             send_sem=dss.at[2 + k], recv_sem=drs.at[2 + k], device_id=sib, device_id_type=MESH,
         )
 
-    def mix(base, i):
+    def mix(base, i, blocks):
         r = pl.ds(mul(base, 256), 256)
-        left = jnp.concatenate([so[b, r, :] for b in range(4)], axis=1)
-        return dot(left, jnp.concatenate([mo[i * 4 + q] for q in range(4)], axis=1))
+        left = jnp.concatenate([so[b, r, :] for b in blocks], axis=1)
+        right = jnp.concatenate(
+            [
+                jnp.concatenate([mo[i * 4 + q, pl.ds(mul(b * 128, 128), 128), :] for b in blocks], axis=0)
+                for q in range(4)
+            ],
+            axis=1,
+        )
+        return dot(left, right)
+
+    near = (x, lax.rem(x + 3, 4))
+    far = (lax.rem(x + 1, 4), lax.rem(x + 2, 4))
 
     for k in range(2):
         @pl.loop(0, 4)
         def _(i):
-            msend[k * 256 : k * 256 + 256, pl.ds(mul(i * 512, 512), 512)] = mix(
-                theirs + k * 256, i
-            ).astype(BF16)
+            at = (slice(k * 256, k * 256 + 256), pl.ds(mul(i * 512, 512), 512))
+            mtheir[at] = mix(theirs + k * 256, i, near)
+            mown[at] = mix(mine + k * 256, i, near)
+
+    g_in1.step(6)
+    g_wd.own(first=False)
+    g_in2.step(4)
+    g_in2.step(5)
+    g_in2.step(6)
+    r_mo.far()
+    r_so.far()
+    g_wd.step(4)
+    g_wd.step(3)
+    for k in range(2):
+        @pl.loop(0, 4)
+        def _(i):
+            at = (slice(k * 256, k * 256 + 256), pl.ds(mul(i * 512, 512), 512))
+            msend[at] = (mtheir[at] + mix(theirs + k * 256, i, far)).astype(BF16)
 
         mix_copy(k).start()
     for k in range(2):
         @pl.loop(0, 4)
         def _(i):
-            mown[k * 256 : k * 256 + 256, pl.ds(mul(i * 512, 512), 512)] = mix(mine + k * 256, i)
-
-    g_in2.step(4, 5, 6)
-    g_wd.step(0, 1)
+            at = (slice(k * 256, k * 256 + 256), pl.ds(mul(i * 512, 512), 512))
+            mown[at] = mown[at] + mix(mine + k * 256, i, far)
+
+    g_in2.step(2)
+    g_wd.step(5)
     for k in range(2):
         mix_copy(k).wait_recv()
 
@@ -406,9 +474,6 @@
 
         fn_copy(k, mine).start()
 
-    g_in1.rest()
-    g_wd.step(2, 3)
-
     row = lax.broadcasted_iota(jnp.int32, (SEQ, 256), 0)
     lane2 = lax.broadcasted_iota(jnp.int32, (SEQ, 128), 1)
 
@@ -425,46 +490,35 @@
         )
         return lax.dot_general(a, w, (((1,), (1,)), ((), ())), preferred_element_type=F32)
 
-    def hidden(seq, tile):
-        r = pl.ds(mul(seq * SEQ, SEQ), SEQ)
-        p = dot_t(fn[r, :], pl.ds(mul(tile * 128, 128), 128))
-        q = conv(p, taps[:, pl.ds(mul(tile * 256, 256), 256)])
-        hid[r, pl.ds(mul(tile * 128, 128), 128)] = (
-            jax.nn.silu(q[:, :128]) * q[:, 128:]
-        ).astype(BF16)
-
-    def hidden_last(seq):
-        r = pl.ds(mul(seq * SEQ, SEQ), SEQ)
-        p = dot_t(fn[r, :], pl.ds(640, 64))
-        q = conv(p, taps[:, 1280:1408])
-        h = jax.nn.silu(q) * pltpu.roll(q, 64, 1)
-        hid[r, 640:768] = jnp.where(lane2 < 64, h, 0.0).astype(BF16)
-
-    own_seq = c * 2
-    other_seq = (1 - c) * 2
-
-    def part1(first):
-        @pl.loop(0, 6)
+    def tiles(first, start, stop):
+        @pl.loop(start, stop)
         def _(i):
-            hidden(first + i // 3, i % 3)
-
-    def part2(first):
-        @pl.loop(0, 4)
-        def _(i):
-            hidden(first + i // 2, 3 + i % 2)
-
-        @pl.loop(0, 2)
-        def _(i):
-            hidden_last(first + i)
-
-    part1(own_seq)
-    g_wd.step(4, 5, 6)
+            p = dot_t(fn[pl.ds(mul(first * SEQ, SEQ), 2 * SEQ), :], pl.ds(mul(i * 128, 128), 128))
+            for h in range(2):
+                q = conv(p[h * SEQ : h * SEQ + SEQ], taps[:, pl.ds(mul(i * 256, 256), 256)])
+                hid[pl.ds(mul((first + h) * SEQ, SEQ), SEQ), pl.ds(mul(i * 128, 128), 128)] = (
+                    jax.nn.silu(q[:, :128]) * q[:, 128:]
+                ).astype(BF16)
+
+    def last(first):
+        p = dot_t(fn[pl.ds(mul(first * SEQ, SEQ), 2 * SEQ), :], pl.ds(640, 64))
+        for k in range(2):
+            q = conv(p[k * SEQ : k * SEQ + SEQ], taps[:, 1280:1408])
+            h = jax.nn.silu(q) * pltpu.roll(q, 64, 1)
+            hid[pl.ds(mul((first + k) * SEQ, SEQ), SEQ), 640:768] = jnp.where(
+                lane2 < 64, h, 0.0
+            ).astype(BF16)
+
+    g_wd.step(2)
+    g_in1.rest()
+    tiles(c * 2, 0, 3)
+    g_wd.step(6)
     for k in range(2):
         fn_copy(k, (1 - c) * 512).wait_recv()
-    part1(other_seq)
+    tiles((1 - c) * 2, 0, 3)
     g_in2.rest()
-    part2(own_seq)
-    part2(other_seq)
+    tiles(0, 3, 5)
+    last(0)
     g_wd.rest()
 
     hops = (2, 1, 3, 0)
@@ -519,14 +573,16 @@
         x_copies[slot].start()
 
     down_theirs(0, 0)
+    down_theirs(2, 0)
+    tiles(2, 3, 5)
+    fill(0, 0, 0)
+    fill(2, 0, 3)
+    last(2)
     down_theirs(0, 1)
     down_theirs(1, 1)
-    fill(0, 0, 0)
+    down_theirs(1, 0)
     fill(0, 1, 1)
-    down_theirs(2, 0)
     fill(1, 1, 2)
-    fill(2, 0, 3)
-    down_theirs(1, 0)
     down_theirs(2, 1)
     down_theirs(3, 0)
     down_theirs(3, 1)
@@ -595,7 +651,7 @@
     return pl.pallas_call(
         kernel,
         out_shape=jax.ShapeDtypeStruct((ROWS, 256), BF16),
-        in_specs=[hbm] * 7 + [vmem] * 7,
+        in_specs=[hbm] * 14,
         out_specs=vmem,
         scratch_shapes=[
             V((ROWS, D), BF16),
@@ -612,8 +668,16 @@
             V((16, 128), F32),
             V((4, ROWS, 128), BF16),
             V((8, 1408), F32),
+            V((1, 128), F32),
+            V((2, 128, 128), BF16),
+            V((2, 128), F32),
+            V((1, D), F32),
+            V((3, 704), F32),
+            V((3, 704), F32),
+            V((1, D), F32),
             V((512, D), BF16),
             V((512, D), BF16),
+            V((512, D), F32),
             V((512, D), F32),
             V((ROWS, D), BF16),
             V((ROWS, 768), BF16),
@@ -623,11 +687,11 @@
             V((ROWS, 256), BF16),
             V((2, ROWS, 256), BF16),
             V((ROWS, 256), F32),
-            DMA((7,)),
+            DMA((14,)),
             DMA((5, 2, 16)),
             DMA((5, 2, 16)),
-            DMA((2, 6)),
-            DMA((2, 6)),
+            DMA((2, 8)),
+            DMA((2, 8)),
             DMA((2, 8)),
             DMA((2, 8)),
             DMA((4,)),

time: 111 us -> 98.8 us (0.89)
  Pallas kernels: 109 us -> 96.8 us
    pallas_call x1, Pallas kernels: 109 us -> 96.8 us  [per_device(): pl.pallas_call(kernel, out_shape=jax.ShapeDtypeStruct((ROWS, 256), BF16),...]
where the time goes in v3:
time: 98.8 us; the launch traced here: 98.6 us
  Pallas kernels  96.8 us (98%)
  local copies, waits for them, and re-layouts  1.87 us (2%)
    pallas_call x1, Pallas kernels, per_device(): pl.pallas_call(kernel, out_shape=jax.ShapeDtypeStruct((ROWS, 256), BF16),...  96.8 us

profile of v3, /device:TPU:1, one launch (start us, length us, event | category | flops | bytes accessed | tf_op | source)
XLA Modules:
  0.0 98.6 jit_solution(14821399096081539978)
XLA Ops:
  0.0 96.8 %shard_map.136 = bf16[1024,256]{1,0:T(8,128)(2,1)} custom-call(bf16[1024,2048]{1,0:T(8,128)(2,1)} %tok_h.1, bf16[128,128]{1,0:T(8,128)(2,1)} %gate_h.1, bf16[128,128]{1,0:T(8,128)(2,1)} %value_h.1, bf16[128,128]{1,0:T(8,128)(2,1)} %mo_h.1, bf16[704,128]{1,0:T(8,128)(2,1)} %bitcast.5, bf16[704,128]{1,0:T(8,128)(2,1)} %bitcast.6, bf16[704,128]{1,0:T(8,128)(2,1)} %wd_h.1, ...), custom_call_target="tpu_custom_call" | custom-call | tf_op jit(solution)/shard_map/pallas_call | solution.py:651
  96.8 1.9 %copy.16 = bf16[1024,256]{1,0:T(8,128)(2,1)} copy(bf16[1024,256]{1,0:T(8,128)(2,1)} %shard_map.136) | data formatting | bytes 1048576

commit v4 on v3

--- a/solution.py
+++ b/solution.py
@@ -188,9 +188,12 @@
 
 
 class Stats:
-    def __init__(self, ref, x, c, send_sem, recv_sem):
-        self.ref, self.x, self.c = ref, x, c
+    def __init__(self, ref, x, c, send_sem, recv_sem, half=None):
+        self.ref, self.x, self.c, self.half = ref, x, c, half
         self.send_sem, self.recv_sem = send_sem, recv_sem
+
+    def at(self, k):
+        return k if self.half is None else (k, self.half)
 
     def copies(self):
         out = []
@@ -198,8 +201,8 @@
             dx, dc = k // 2, k % 2
             out.append(
                 pltpu.make_async_remote_copy(
-                    src_ref=self.ref.at[0],
-                    dst_ref=self.ref.at[k],
+                    src_ref=self.ref.at[self.at(0)],
+                    dst_ref=self.ref.at[self.at(k)],
                     send_sem=self.send_sem.at[k],
                     recv_sem=self.recv_sem.at[k],
                     device_id={"x": lax.rem(self.x + dx, 4), "c": lax.rem(self.c + dc, 2)},
@@ -215,9 +218,9 @@
     def total(self):
         for c in self.copies():
             c.wait_recv()
-        total = self.ref[0]
+        total = self.ref[self.at(0)]
         for k in range(1, 8):
-            total = total + self.ref[k]
+            total = total + self.ref[self.at(k)]
         return total
 
     def sent(self):
@@ -233,7 +236,7 @@
     tok_h, gate_h, value_h, mo_h, fg_h, fu_h, wd_h, gain_h, wsp_h, bias_h, g1_h, tg_h, tu_h, g2_h,
     out,
     tok, wgt, wvl, mo, wfg, wfu, wd, ga, va, st1, st2, tot, so, taps, gain, wsp, bias, g1, taps_g, taps_u, g2,
-    msend, mrecv, mown, mtheir, fn, hid, dsend, drecv, xs, xr2, xr1, acc,
+    msend, mrecv, mown, mtheir, fn, hid, dsend, drecv, xs, xr, pend, acc,
     lsem, psend, precv, rsend, rrecv, ssend, srecv, dss, drs, dds, ddr, xss, xrs,
 ):
     z, y = lax.axis_index("z"), lax.axis_index("y")
@@ -268,12 +271,12 @@
     r_mo = RingGather(mo_ring, x, rsend.at[0], rrecv.at[0], 2)
     r_so = RingGather(so_ring, x, rsend.at[1], rrecv.at[1], 1)
     g_gv = PlaneGather(gv_block, pos, psend.at[0], precv.at[0], 0)
-    g_mo = PlaneGather(mo_block, pos, psend.at[1], precv.at[1], 1, r_mo.piece)
+    g_mo = PlaneGather(mo_block, pos, psend.at[1], precv.at[1], 0, r_mo.piece)
     g_in1 = PlaneGather(in1_block, pos, psend.at[2], precv.at[2], 0)
     g_in2 = PlaneGather(in2_block, pos, psend.at[3], precv.at[3], 1)
-    g_wd = PlaneGather(wd_block, pos, psend.at[4], precv.at[4], 0)
+    g_wd = PlaneGather(wd_block, pos, psend.at[4], precv.at[4], 1)
     s1 = Stats(st1, x, c, ssend.at[0], srecv.at[0])
-    s2 = Stats(st2, x, c, ssend.at[1], srecv.at[1])
+    s2 = [Stats(st2, x, c, ssend.at[1 + h], srecv.at[1 + h], h) for h in range(2)]
 
     rows_f = pl.ds(mul(f * 128, 128), 128)
     loads = [
@@ -320,32 +323,33 @@
 
     g_mo.own(second=False)
     g_gv.own(second=False)
+    g_mo.own(first=False)
     loads[3].wait()
     loads[4].wait()
     g_in1.own(second=False)
-    g_gv.own(first=False)
     g_mo.step(0)
     g_mo.step(1)
     g_gv.step(1)
     g_gv.step(0)
-    g_mo.own(first=False)
-    g_in1.step(1)
-    g_gv.step(5)
+    g_gv.own(first=False)
+    g_in2.own(second=False)
     g_mo.step(3)
-    g_mo.step(5)
     g_gv.step(3)
-    g_gv.step(4)
-    g_mo.step(2)
-    g_mo.step(4)
-    g_in2.own(second=False)
-    g_gv.step(2)
-    g_mo.step(6)
-    g_gv.step(6)
-    g_in1.step(0)
     loads[5].wait()
     g_wd.own(second=False)
+    g_gv.step(4)
+    g_mo.step(5)
+    g_mo.step(4)
+    g_gv.step(2)
+    g_mo.step(2)
+    g_mo.step(6)
+    g_gv.step(5)
+    g_gv.step(6)
+    g_in1.own(first=False)
+    g_in1.step(0)
+    g_in1.step(1)
+    g_in2.step(1)
     g_mo.rest()
-    g_in1.own(first=False)
     g_gv.rest()
     loads[6].wait()
     @pl.loop(0, 4)
@@ -363,8 +367,10 @@
     s1.start()
     g_in2.step(0)
     r_mo.forward(0)
-    g_in2.step(1)
+    g_in1.step(4)
     g_wd.step(0)
+    g_in1.step(5)
+    g_wd.step(1)
     tot[...] = s1.total()
     lane = lax.broadcasted_iota(jnp.int32, (128, 128), 1)
     low = lax.broadcasted_iota(jnp.int32, (128, 128), 0) >= lane
@@ -385,17 +391,16 @@
 
         r_so.own(part)
 
-    g_wd.step(1)
-    r_mo.forward(1)
     g_in1.step(3)
     g_in2.step(3)
     g_in2.own(first=False)
-    g_in1.step(2)
-    g_in1.step(4)
+    r_mo.forward(1)
+    g_wd.own(first=False)
     r_so.forward(0)
     r_mo.near()
     r_so.near()
-    g_in1.step(5)
+    g_wd.step(4)
+    g_in2.step(4)
     theirs = (1 - c) * 512
     mine = c * 512
 
@@ -435,15 +440,14 @@
             mtheir[at] = mix(theirs + k * 256, i, near)
             mown[at] = mix(mine + k * 256, i, near)
 
+    g_in1.step(2)
     g_in1.step(6)
-    g_wd.own(first=False)
-    g_in2.step(4)
     g_in2.step(5)
     g_in2.step(6)
+    g_wd.step(5)
+    g_wd.step(3)
     r_mo.far()
     r_so.far()
-    g_wd.step(4)
-    g_wd.step(3)
     for k in range(2):
         @pl.loop(0, 4)
         def _(i):
@@ -458,7 +462,6 @@
             mown[at] = mown[at] + mix(mine + k * 256, i, far)
 
     g_in2.step(2)
-    g_wd.step(5)
     for k in range(2):
         mix_copy(k).wait_recv()
 
@@ -512,133 +515,159 @@
     g_wd.step(2)
     g_in1.rest()
     tiles(c * 2, 0, 3)
-    g_wd.step(6)
     for k in range(2):
         fn_copy(k, (1 - c) * 512).wait_recv()
     tiles((1 - c) * 2, 0, 3)
+    g_wd.step(6)
     g_in2.rest()
     tiles(0, 3, 5)
     last(0)
     g_wd.rest()
 
     hops = (2, 1, 3, 0)
-
-    def dd_copy(k, h):
-        r = pl.ds(h * 512, 512)
+    groups = ((0, 1), (1, 2), (3, 1))
+
+    def seq_rows(s):
+        return pl.ds(s * SEQ, SEQ)
+
+    def dd_copy(g, s):
+        ref = (pl.ds(groups[g][0], groups[g][1]), seq_rows(s), slice(None))
         return pltpu.make_async_remote_copy(
-            src_ref=dsend.at[k, r, :], dst_ref=drecv.at[k, r, :],
-            send_sem=dds.at[k, h], recv_sem=ddr.at[k, h], device_id=sib, device_id_type=MESH,
-        )
-
-    def down(k, i, parity):
-        b = (lax.rem(x + hops[k], 4) * 2 + parity) * 2
-        return dot(
-            hid[pl.ds(mul(i * 256, 256), 256), :], jnp.concatenate([wd[b], wd[b + 1]], axis=1)
-        )
-
-    def down_theirs(k, h):
-        @pl.loop(h * 2, h * 2 + 2)
-        def _(i):
-            dsend[k, pl.ds(mul(i * 256, 256), 256), :] = down(k, i, 1 - c).astype(BF16)
-
-        dd_copy(k, h).start()
-
-    def x_copy(slot, src, dst, step):
+            src_ref=dsend.at[ref], dst_ref=drecv.at[ref],
+            send_sem=dds.at[g, s], recv_sem=ddr.at[g, s], device_id=sib, device_id_type=MESH,
+        )
+
+    def down(g, s, parity):
+        cols = []
+        for k in range(groups[g][0], groups[g][0] + groups[g][1]):
+            b = (lax.rem(x + hops[k], 4) * 2 + parity) * 2
+            cols += [wd[b], wd[b + 1]]
+        return dot(hid[seq_rows(s), :], jnp.concatenate(cols, axis=1))
+
+    def theirs_of(g, s):
+        p = down(g, s, 1 - c)
+        for i in range(groups[g][1]):
+            dsend[groups[g][0] + i, seq_rows(s), :] = p[:, i * 256 : i * 256 + 256].astype(BF16)
+        dd_copy(g, s).start()
+
+    def ours(g, s):
+        dd_copy(g, s).wait_recv()
+        p = down(g, s, c)
+        return [
+            p[:, i * 256 : i * 256 + 256] + drecv[groups[g][0] + i, seq_rows(s), :].astype(F32)
+            for i in range(groups[g][1])
+        ]
+
+    def x_copy(i, s):
         return pltpu.make_async_remote_copy(
-            src_ref=src, dst_ref=dst, send_sem=xss.at[slot], recv_sem=xrs.at[slot],
-            device_id={"x": lax.rem(x + 4 + step, 4)}, device_id_type=MESH,
-        )
-
-    up, lo = pl.ds(0, 512), pl.ds(512, 512)
-    x_copies = (
-        x_copy(0, xs.at[0, up], xr2.at[up], 1),
-        x_copy(1, xs.at[0, lo], xr2.at[lo], -1),
-        x_copy(2, xs.at[1, lo], xr1.at[0, lo], 1),
-        x_copy(3, xs.at[2, up], xr1.at[1, up], -1),
-        x_copy(4, xs.at[1, up], xr1.at[0, up], 1),
-        x_copy(5, xs.at[2, lo], xr1.at[1, lo], -1),
-    )
-
-    def fill(k, h, slot, extra=False):
-        dd_copy(k, h).wait_recv()
-
-        @pl.loop(h * 2, h * 2 + 2)
-        def _(i):
-            r = pl.ds(mul(i * 256, 256), 256)
-            v = down(k, i, c) + drecv[k, r, :].astype(F32)
-            if extra:
-                v = v + xr2[r, :].astype(F32)
-            xs[k, r, :] = v.astype(BF16)
-
-        x_copies[slot].start()
-
-    down_theirs(0, 0)
-    down_theirs(2, 0)
-    tiles(2, 3, 5)
-    fill(0, 0, 0)
-    fill(2, 0, 3)
+            src_ref=xs.at[i, seq_rows(s), :], dst_ref=xr.at[i, seq_rows(s), :],
+            send_sem=xss.at[i, s], recv_sem=xrs.at[i, s],
+            device_id={"x": lax.rem(x + (1 if i % 2 == 0 else 3), 4)}, device_id_type=MESH,
+        )
+
+    def put(i, s, v):
+        xs[i, seq_rows(s), :] = v.astype(BF16)
+        x_copy(i, s).start()
+
+    def got(i, s):
+        return xr[i, seq_rows(s), :].astype(F32)
+
+    def far_out(s):
+        v = ours(0, s)[0]
+        put(0, s, v[:, :128])
+        put(1, s, v[:, 128:])
+
+    def near_out(s):
+        p, m = ours(1, s)
+        put(2, s, p[:, 128:])
+        put(3, s, m[:, :128])
+        pend[0, seq_rows(s), :] = p[:, :128]
+        pend[1, seq_rows(s), :] = m[:, 128:]
+
+    def joined_out(s):
+        for i in range(2):
+            x_copy(i, s).wait_recv()
+            put(4 + i, s, pend[i, seq_rows(s), :] + got(i, s))
+
+    def own_out(s):
+        acc[seq_rows(s), :] = ours(2, s)[0] + SCALE * fn[
+            seq_rows(s), pl.ds(mul(j * 256, 256), 256)
+        ].astype(F32)
+
+    def finish(s):
+        for i in range(2, 6):
+            x_copy(i, s).wait_recv()
+        a = acc[seq_rows(s), :128] + (got(4, s) + got(3, s))
+        b = acc[seq_rows(s), 128:] + (got(2, s) + got(5, s))
+        acc[seq_rows(s), :128] = a
+        acc[seq_rows(s), 128:] = b
+        half, row = s // 2, s % 2 * 2
+        total, square = a + b, a * a + b * b
+        for i in range(2):
+            r = slice(i * 128, i * 128 + 128)
+            st2[0, half, row + i : row + i + 1, :] = jnp.sum(total[r].T, axis=0, keepdims=True)
+            st2[0, half, row + i + 4 : row + i + 5, :] = jnp.sum(square[r].T, axis=0, keepdims=True)
+
+    def normed(h, sums):
+        for i in range(4):
+            r = slice(h * 512 + i * 128, h * 512 + i * 128 + 128)
+            mean = spread(sums[i : i + 1, :] * (1.0 / D))
+            square = spread(sums[i + 4 : i + 5, :] * (1.0 / D))
+            inv = lax.rsqrt(square - mean * mean + EPS)
+            for q in range(2):
+                cols = slice(q * 128, q * 128 + 128)
+                out[r, cols] = ((acc[r, cols] - mean) * inv * gain2[:, cols]).astype(BF16)
+
+    theirs_of(0, 0)
+    theirs_of(1, 0)
+    theirs_of(0, 1)
+    theirs_of(1, 1)
+    far_out(0)
+    near_out(0)
+    far_out(1)
+    near_out(1)
+    tiles(2, 3, 4)
+    tiles(2, 4, 5)
     last(2)
-    down_theirs(0, 1)
-    down_theirs(1, 1)
-    down_theirs(1, 0)
-    fill(0, 1, 1)
-    fill(1, 1, 2)
-    down_theirs(2, 1)
-    down_theirs(3, 0)
-    down_theirs(3, 1)
-    x_copies[0].wait_recv()
-    fill(1, 0, 4, True)
-    x_copies[1].wait_recv()
-    fill(2, 1, 5, True)
-    for h in range(2):
-        dd_copy(3, h).wait_recv()
-
-        @pl.loop(h * 2, h * 2 + 2)
-        def _(i):
-            r = pl.ds(mul(i * 256, 256), 256)
-            acc[r, :] = (
-                down(3, i, c)
-                + drecv[3, r, :].astype(F32)
-                + SCALE * fn[r, pl.ds(mul(j * 256, 256), 256)].astype(F32)
-            )
-
+    joined_out(0)
+    theirs_of(0, 2)
+    theirs_of(1, 2)
+    theirs_of(0, 3)
+    theirs_of(1, 3)
+    joined_out(1)
+    far_out(2)
+    far_out(3)
+    near_out(2)
+    near_out(3)
+    for s in range(4):
+        theirs_of(2, s)
+    joined_out(2)
+    joined_out(3)
+    for s in range(4):
+        own_out(s)
     for g in (g_gv, g_mo, g_in1, g_in2, g_wd, r_mo, r_so, s1):
         g.sent()
     for k in range(2):
         mix_copy(k).wait_send()
         fn_copy(k, mine).wait_send()
-    for k in range(4):
-        for h in range(2):
-            dd_copy(k, h).wait_send()
-    for k in (2, 3, 4, 5):
-        x_copies[k].wait_recv()
-
-    @pl.loop(0, 8)
-    def _(n):
-        r = pl.ds(mul(n * 128, 128), 128)
-        v = acc[r, :] + (xr1[0, r, :].astype(F32) + xr1[1, r, :].astype(F32))
-        acc[r, :] = v
-        a, b = v[:, :128], v[:, 128:]
-        st2[0, pl.ds(n, 1), :] = jnp.sum((a + b).T, axis=0, keepdims=True)
-        st2[0, pl.ds(n + 8, 1), :] = jnp.sum((a * a + b * b).T, axis=0, keepdims=True)
-
-    s2.start()
+    for g in range(3):
+        for s in range(4):
+            dd_copy(g, s).wait_send()
     gain2 = g2[:, pl.ds(mul(j * 256, 256), 256)]
-    for k in range(6):
-        x_copies[k].wait_send()
-    tot[...] = s2.total()
-
-    @pl.loop(0, 8)
-    def _(n):
-        r = pl.ds(mul(n * 128, 128), 128)
-        mean = spread(tot[pl.ds(n, 1), :] * (1.0 / D))
-        square = spread(tot[pl.ds(n + 8, 1), :] * (1.0 / D))
-        inv = lax.rsqrt(square - mean * mean + EPS)
-        for h in range(2):
-            cols = slice(h * 128, h * 128 + 128)
-            out[r, cols] = ((acc[r, cols] - mean) * inv * gain2[:, cols]).astype(BF16)
-
-    s2.sent()
+    finish(0)
+    finish(1)
+    s2[0].start()
+    finish(2)
+    finish(3)
+    s2[1].start()
+    normed(0, s2[0].total())
+    for i in range(6):
+        for s in range(4):
+            x_copy(i, s).wait_send()
+    last_sums = s2[1].total()
+    normed(1, last_sums)
+    for s in s2:
+        s.sent()
 
 
 def per_device(
@@ -664,7 +693,7 @@
             V((ROWS, 128), F32),
             V((ROWS, 128), F32),
             V((8, 16, 128), F32),
-            V((8, 16, 128), F32),
+            V((8, 2, 8, 128), F32),
             V((16, 128), F32),
             V((4, ROWS, 128), BF16),
             V((8, 1408), F32),
@@ -683,23 +712,23 @@
             V((ROWS, 768), BF16),
             V((4, ROWS, 256), BF16),
             V((4, ROWS, 256), BF16),
-            V((3, ROWS, 256), BF16),
-            V((ROWS, 256), BF16),
-            V((2, ROWS, 256), BF16),
+            V((6, ROWS, 128), BF16),
+            V((6, ROWS, 128), BF16),
+            V((2, ROWS, 128), F32),
             V((ROWS, 256), F32),
             DMA((14,)),
             DMA((5, 2, 16)),
             DMA((5, 2, 16)),
             DMA((2, 8)),
             DMA((2, 8)),
-            DMA((2, 8)),
-            DMA((2, 8)),
+            DMA((3, 8)),
+            DMA((3, 8)),
             DMA((4,)),
             DMA((4,)),
-            DMA((4, 2)),
-            DMA((4, 2)),
-            DMA((6,)),
-            DMA((6,)),
+            DMA((3, 4)),
+            DMA((3, 4)),
+            DMA((6, 4)),
+            DMA((6, 4)),
         ],
         compiler_params=pltpu.CompilerParams(
             collective_id=0, has_side_effects=True, vmem_limit_bytes=60 * 1024 * 1024

time: 98.8 us -> 95.5 us (0.967)
  Pallas kernels: 96.8 us -> 93.5 us
    pallas_call x1, Pallas kernels: 96.8 us -> 93.5 us  [per_device(): pl.pallas_call(kernel, out_shape=jax.ShapeDtypeStruct((ROWS, 256), BF16),...]
where the time goes in v4:
time: 95.5 us; the launch traced here: 95.4 us
  Pallas kernels  93.5 us (98%)
  local copies, waits for them, and re-layouts  1.87 us (2%)
    pallas_call x1, Pallas kernels, per_device(): pl.pallas_call(kernel, out_shape=jax.ShapeDtypeStruct((ROWS, 256), BF16),...  93.5 us

profile of v4, /device:TPU:1, one launch (start us, length us, event | category | flops | bytes accessed | tf_op | source)
XLA Modules:
  0.0 95.4 jit_solution(10099034241062656530)
XLA Ops:
  0.0 93.5 %shard_map.136 = bf16[1024,256]{1,0:T(8,128)(2,1)} custom-call(bf16[1024,2048]{1,0:T(8,128)(2,1)} %tok_h.1, bf16[128,128]{1,0:T(8,128)(2,1)} %gate_h.1, bf16[128,128]{1,0:T(8,128)(2,1)} %value_h.1, bf16[128,128]{1,0:T(8,128)(2,1)} %mo_h.1, bf16[704,128]{1,0:T(8,128)(2,1)} %bitcast.5, bf16[704,128]{1,0:T(8,128)(2,1)} %bitcast.6, bf16[704,128]{1,0:T(8,128)(2,1)} %wd_h.1, ...), custom_call_target="tpu_custom_call" | custom-call | tf_op jit(solution)/shard_map/pallas_call | solution.py:680
  93.5 1.9 %copy.16 = bf16[1024,256]{1,0:T(8,128)(2,1)} copy(bf16[1024,256]{1,0:T(8,128)(2,1)} %shard_map.136) | data formatting | bytes 1048576

commit v5 on v4

--- a/solution.py
+++ b/solution.py
@@ -283,8 +283,8 @@
         pltpu.make_async_copy(gate_h, wgt.at[rows_f, :], lsem.at[0]),
         pltpu.make_async_copy(value_h, wvl.at[rows_f, :], lsem.at[1]),
         pltpu.make_async_copy(mo_h, mo.at[f, pl.ds(mul(x * 128, 128), 128), :], lsem.at[2]),
-        pltpu.make_async_copy(fg_h, wfg.at[f], lsem.at[3]),
-        pltpu.make_async_copy(fu_h, wfu.at[f], lsem.at[4]),
+        pltpu.make_async_copy(fg_h, wfg.at[f, pl.ds(0, 704), :], lsem.at[3]),
+        pltpu.make_async_copy(fu_h, wfu.at[f, pl.ds(0, 704), :], lsem.at[4]),
         pltpu.make_async_copy(wd_h, wd.at[f, pl.ds(0, 704), :], lsem.at[5]),
         pltpu.make_async_copy(tok_h, tok, lsem.at[6]),
     ]
@@ -307,16 +307,20 @@
     ]
     for p in peers:
         pl.semaphore_signal(barrier, inc=1, device_id=p, device_id_type=MESH)
-    for b in range(16):
-        wd[b, 704:768, :] = jnp.zeros((64, 128), BF16)
+    for buf in (wd, wfg, wfu):
+        @pl.loop(0, 16)
+        def _(b):
+            buf[b, 704:768, :] = jnp.zeros((64, 128), BF16)
+
     for l in small:
         l.wait()
     for i in range(5):
         t = slice(i * 128, i * 128 + 128)
         taps[0:3, i * 256 : i * 256 + 128] = taps_g[:, t]
         taps[0:3, i * 256 + 128 : i * 256 + 256] = taps_u[:, t]
+    taps[:, 1280:1536] = jnp.zeros((8, 256), F32)
     taps[0:3, 1280:1344] = taps_g[:, 640:704]
-    taps[0:3, 1344:1408] = taps_u[:, 640:704]
+    taps[0:3, 1408:1472] = taps_u[:, 640:704]
     for k in range(3):
         loads[k].wait()
     pl.semaphore_wait(barrier, len(peers))
@@ -378,18 +382,19 @@
     w1 = jnp.where(low, wsp[1], jnp.zeros((128, 128), BF16))
     shift = jnp.where(lane < 64, spread(bias[0:1, :]), spread(bias[1:2, :]))
 
-    for part in range(2):
-        @pl.loop(part * 4, part * 4 + 4)
-        def _(n):
-            r = pl.ds(mul(n * 128, 128), 128)
-            mean = spread(tot[pl.ds(n, 1), :] * (1.0 / SG_WIDTH))
-            square = spread(tot[pl.ds(n + 8, 1), :] * (1.0 / SG_WIDTH))
-            inv = lax.rsqrt(square - mean * mean + EPS)
-            vn = ((va[r, :] - mean) * inv * gain[...]).astype(BF16)
-            mixed = jnp.where(lane < 64, dot(w0, vn), dot(w1, vn)) + shift
-            so[x, r, :] = (ga[r, :] * mixed).astype(BF16)
-
-        r_so.own(part)
+    @pl.loop(0, 8)
+    def _(n):
+        r = pl.ds(mul(n * 128, 128), 128)
+        mean = spread(tot[pl.ds(n, 1), :] * (1.0 / SG_WIDTH))
+        square = spread(tot[pl.ds(n + 8, 1), :] * (1.0 / SG_WIDTH))
+        inv = lax.rsqrt(square - mean * mean + EPS)
+        vn = ((va[r, :] - mean) * inv * gain[...]).astype(BF16)
+        mixed = jnp.where(lane < 64, dot(w0, vn), dot(w1, vn)) + shift
+        so[x, r, :] = (ga[r, :] * mixed).astype(BF16)
+        for part in range(2):
+            @pl.when(n == part * 4 + 3)
+            def _():
+                r_so.own(part)
 
     g_in1.step(3)
     g_in2.step(3)
@@ -433,12 +438,13 @@
     near = (x, lax.rem(x + 3, 4))
     far = (lax.rem(x + 1, 4), lax.rem(x + 2, 4))
 
-    for k in range(2):
-        @pl.loop(0, 4)
-        def _(i):
-            at = (slice(k * 256, k * 256 + 256), pl.ds(mul(i * 512, 512), 512))
-            mtheir[at] = mix(theirs + k * 256, i, near)
-            mown[at] = mix(mine + k * 256, i, near)
+    def mix_at(i):
+        return pl.ds(mul(i // 4 * 256, 256), 256), pl.ds(mul(i % 4 * 512, 512), 512)
+
+    @pl.loop(0, 8)
+    def _(i):
+        mtheir[mix_at(i)] = mix(theirs + i // 4 * 256, i % 4, near)
+        mown[mix_at(i)] = mix(mine + i // 4 * 256, i % 4, near)
 
     g_in1.step(2)
     g_in1.step(6)
@@ -448,37 +454,40 @@
     g_wd.step(3)
     r_mo.far()
     r_so.far()
-    for k in range(2):
-        @pl.loop(0, 4)
-        def _(i):
-            at = (slice(k * 256, k * 256 + 256), pl.ds(mul(i * 512, 512), 512))
-            msend[at] = (mtheir[at] + mix(theirs + k * 256, i, far)).astype(BF16)
-
-        mix_copy(k).start()
-    for k in range(2):
-        @pl.loop(0, 4)
-        def _(i):
-            at = (slice(k * 256, k * 256 + 256), pl.ds(mul(i * 512, 512), 512))
-            mown[at] = mown[at] + mix(mine + k * 256, i, far)
+    @pl.loop(0, 8)
+    def _(i):
+        p = mix(theirs + i // 4 * 256, i % 4, far)
+        msend[mix_at(i)] = (mtheir[mix_at(i)] + p).astype(BF16)
+        for k in range(2):
+            @pl.when(i == k * 4 + 3)
+            def _():
+                mix_copy(k).start()
+
+    @pl.loop(0, 8)
+    def _(i):
+        mown[mix_at(i)] = mown[mix_at(i)] + mix(mine + i // 4 * 256, i % 4, far)
 
     g_in2.step(2)
-    for k in range(2):
-        mix_copy(k).wait_recv()
-
-        @pl.loop(0, 8)
-        def _(i):
-            r = pl.ds(mul(k * 256 + i * 32, 32), 32)
-            g = pl.ds(mul(mine + k * 256 + i * 32, 32), 32)
-            v = SCALE * tok[g, :].astype(F32) + (mown[r, :] + mrecv[r, :].astype(F32))
-            mean = jnp.sum(v, axis=1, keepdims=True) * (1.0 / D)
-            square = jnp.sum(v * v, axis=1, keepdims=True) * (1.0 / D)
-            inv = lax.rsqrt(square - mean * mean + EPS)
-            fn[g, :] = ((v - mean) * inv * g1[...]).astype(BF16)
-
-        fn_copy(k, mine).start()
+    @pl.loop(0, 16)
+    def _(i):
+        for k in range(2):
+            @pl.when(i == k * 8)
+            def _():
+                mix_copy(k).wait_recv()
+
+        r = pl.ds(mul(i * 32, 32), 32)
+        g = pl.ds(mul(mine + i * 32, 32), 32)
+        v = SCALE * tok[g, :].astype(F32) + (mown[r, :] + mrecv[r, :].astype(F32))
+        mean = jnp.sum(v, axis=1, keepdims=True) * (1.0 / D)
+        square = jnp.sum(v * v, axis=1, keepdims=True) * (1.0 / D)
+        inv = lax.rsqrt(square - mean * mean + EPS)
+        fn[g, :] = ((v - mean) * inv * g1[...]).astype(BF16)
+        for k in range(2):
+            @pl.when(i == k * 8 + 7)
+            def _():
+                fn_copy(k, mine).start()
 
     row = lax.broadcasted_iota(jnp.int32, (SEQ, 256), 0)
-    lane2 = lax.broadcasted_iota(jnp.int32, (SEQ, 128), 1)
 
     def conv(p, t):
         n = p.shape[1]
@@ -493,42 +502,41 @@
         )
         return lax.dot_general(a, w, (((1,), (1,)), ((), ())), preferred_element_type=F32)
 
-    def tiles(first, start, stop):
-        @pl.loop(start, stop)
-        def _(i):
-            p = dot_t(fn[pl.ds(mul(first * SEQ, SEQ), 2 * SEQ), :], pl.ds(mul(i * 128, 128), 128))
-            for h in range(2):
-                q = conv(p[h * SEQ : h * SEQ + SEQ], taps[:, pl.ds(mul(i * 256, 256), 256)])
-                hid[pl.ds(mul((first + h) * SEQ, SEQ), SEQ), pl.ds(mul(i * 128, 128), 128)] = (
-                    jax.nn.silu(q[:, :128]) * q[:, 128:]
-                ).astype(BF16)
-
-    def last(first):
-        p = dot_t(fn[pl.ds(mul(first * SEQ, SEQ), 2 * SEQ), :], pl.ds(640, 64))
-        for k in range(2):
-            q = conv(p[k * SEQ : k * SEQ + SEQ], taps[:, 1280:1408])
-            h = jax.nn.silu(q) * pltpu.roll(q, 64, 1)
-            hid[pl.ds(mul((first + k) * SEQ, SEQ), SEQ), 640:768] = jnp.where(
-                lane2 < 64, h, 0.0
+    def tile(first, i):
+        p = dot_t(fn[pl.ds(mul(first * SEQ, SEQ), 2 * SEQ), :], pl.ds(mul(i * 128, 128), 128))
+        for h in range(2):
+            q = conv(p[h * SEQ : h * SEQ + SEQ], taps[:, pl.ds(mul(i * 256, 256), 256)])
+            hid[pl.ds(mul((first + h) * SEQ, SEQ), SEQ), pl.ds(mul(i * 128, 128), 128)] = (
+                jax.nn.silu(q[:, :128]) * q[:, 128:]
             ).astype(BF16)
 
     g_wd.step(2)
     g_in1.rest()
-    tiles(c * 2, 0, 3)
-    for k in range(2):
-        fn_copy(k, (1 - c) * 512).wait_recv()
-    tiles((1 - c) * 2, 0, 3)
-    g_wd.step(6)
-    g_in2.rest()
-    tiles(0, 3, 5)
-    last(0)
+    @pl.loop(0, 9)
+    def _(i):
+        @pl.when(i == 3)
+        def _():
+            for k in range(2):
+                fn_copy(k, (1 - c) * 512).wait_recv()
+
+        @pl.when(i == 4)
+        def _():
+            g_wd.step(6)
+
+        @pl.when(i == 6)
+        def _():
+            g_in2.rest()
+
+        q = i // 3
+        tile((1 - q // 2) * (2 * c * (1 - q) + (2 - 2 * c) * q), i % 3 + q // 2 * 3)
+
     g_wd.rest()
 
     hops = (2, 1, 3, 0)
     groups = ((0, 1), (1, 2), (3, 1))
 
     def seq_rows(s):
-        return pl.ds(s * SEQ, SEQ)
+        return pl.ds(mul(s * SEQ, SEQ), SEQ)
 
     def dd_copy(g, s):
         ref = (pl.ds(groups[g][0], groups[g][1]), seq_rows(s), slice(None))
@@ -618,33 +626,45 @@
                 cols = slice(q * 128, q * 128 + 128)
                 out[r, cols] = ((acc[r, cols] - mean) * inv * gain2[:, cols]).astype(BF16)
 
-    theirs_of(0, 0)
-    theirs_of(1, 0)
-    theirs_of(0, 1)
-    theirs_of(1, 1)
-    far_out(0)
-    near_out(0)
-    far_out(1)
-    near_out(1)
-    tiles(2, 3, 4)
-    tiles(2, 4, 5)
-    last(2)
+    @pl.loop(0, 2)
+    def _(s):
+        theirs_of(0, s)
+        theirs_of(1, s)
+
+    @pl.loop(0, 2)
+    def _(s):
+        far_out(s)
+        near_out(s)
+
+    @pl.loop(3, 6)
+    def _(i):
+        tile(2, i)
+
     joined_out(0)
-    theirs_of(0, 2)
-    theirs_of(1, 2)
-    theirs_of(0, 3)
-    theirs_of(1, 3)
+    @pl.loop(2, 4)
+    def _(s):
+        theirs_of(0, s)
+        theirs_of(1, s)
+
     joined_out(1)
-    far_out(2)
-    far_out(3)
-    near_out(2)
-    near_out(3)
-    for s in range(4):
+    @pl.loop(2, 4)
+    def _(s):
+        far_out(s)
+
+    @pl.loop(2, 4)
+    def _(s):
+        near_out(s)
+
+    @pl.loop(0, 4)
+    def _(s):
         theirs_of(2, s)
+
     joined_out(2)
     joined_out(3)
-    for s in range(4):
+    @pl.loop(0, 4)
+    def _(s):
         own_out(s)
+
     for g in (g_gv, g_mo, g_in1, g_in2, g_wd, r_mo, r_so, s1):
         g.sent()
     for k in range(2):
@@ -687,8 +707,8 @@
             V((D, 128), BF16),
             V((D, 128), BF16),
             V((16, 512, 128), BF16),
-            V((16, 704, 128), BF16),
-            V((16, 704, 128), BF16),
+            V((16, 768, 128), BF16),
+            V((16, 768, 128), BF16),
             V((16, 768, 128), BF16),
             V((ROWS, 128), F32),
             V((ROWS, 128), F32),
@@ -696,7 +716,7 @@
             V((8, 2, 8, 128), F32),
             V((16, 128), F32),
             V((4, ROWS, 128), BF16),
-            V((8, 1408), F32),
+            V((8, 1536), F32),
             V((1, 128), F32),
             V((2, 128, 128), BF16),
             V((2, 128), F32),

time: 95.5 us -> 94.3 us (0.987)
  Pallas kernels: 93.5 us -> 92.3 us
    pallas_call x1, Pallas kernels: 93.5 us -> 92.3 us  [per_device(): pl.pallas_call(kernel, out_shape=jax.ShapeDtypeStruct((ROWS, 256), BF16),...]
where the time goes in v5:
time: 94.3 us; the launch traced here: 94.2 us
  Pallas kernels  92.3 us (98%)
  local copies, waits for them, and re-layouts  1.87 us (2%)
    pallas_call x1, Pallas kernels, per_device(): pl.pallas_call(kernel, out_shape=jax.ShapeDtypeStruct((ROWS, 256), BF16),...  92.3 us

profile of v5, /device:TPU:1, one launch (start us, length us, event | category | flops | bytes accessed | tf_op | source)
XLA Modules:
  0.0 94.2 jit_solution(16358995576815328545)
XLA Ops:
  0.0 92.3 %shard_map.136 = bf16[1024,256]{1,0:T(8,128)(2,1)} custom-call(bf16[1024,2048]{1,0:T(8,128)(2,1)} %tok_h.1, bf16[128,128]{1,0:T(8,128)(2,1)} %gate_h.1, bf16[128,128]{1,0:T(8,128)(2,1)} %value_h.1, bf16[128,128]{1,0:T(8,128)(2,1)} %mo_h.1, bf16[704,128]{1,0:T(8,128)(2,1)} %bitcast.5, bf16[704,128]{1,0:T(8,128)(2,1)} %bitcast.6, bf16[704,128]{1,0:T(8,128)(2,1)} %wd_h.1, ...), custom_call_target="tpu_custom_call" | custom-call | tf_op jit(solution)/shard_map/pallas_call | solution.py:700
  92.3 1.9 %copy.16 = bf16[1024,256]{1,0:T(8,128)(2,1)} copy(bf16[1024,256]{1,0:T(8,128)(2,1)} %shard_map.136) | data formatting | bytes 1048576

commit v6 on v5

--- a/solution.py
+++ b/solution.py
@@ -468,22 +468,22 @@
         mown[mix_at(i)] = mown[mix_at(i)] + mix(mine + i // 4 * 256, i % 4, far)
 
     g_in2.step(2)
-    @pl.loop(0, 16)
+    @pl.loop(0, 8)
     def _(i):
         for k in range(2):
-            @pl.when(i == k * 8)
+            @pl.when(i == k * 4)
             def _():
                 mix_copy(k).wait_recv()
 
-        r = pl.ds(mul(i * 32, 32), 32)
-        g = pl.ds(mul(mine + i * 32, 32), 32)
+        r = pl.ds(mul(i * 64, 64), 64)
+        g = pl.ds(mul(mine + i * 64, 64), 64)
         v = SCALE * tok[g, :].astype(F32) + (mown[r, :] + mrecv[r, :].astype(F32))
         mean = jnp.sum(v, axis=1, keepdims=True) * (1.0 / D)
         square = jnp.sum(v * v, axis=1, keepdims=True) * (1.0 / D)
         inv = lax.rsqrt(square - mean * mean + EPS)
         fn[g, :] = ((v - mean) * inv * g1[...]).astype(BF16)
         for k in range(2):
-            @pl.when(i == k * 8 + 7)
+            @pl.when(i == k * 4 + 3)
             def _():
                 fn_copy(k, mine).start()
 

time: 94.3 us -> 94.3 us (level)
  no operation moved by 1% of the time
where the time goes in v6:
time: 94.3 us; the launch traced here: 94.2 us
  Pallas kernels  92.3 us (98%)
  local copies, waits for them, and re-layouts  1.87 us (2%)
    pallas_call x1, Pallas kernels, per_device(): pl.pallas_call(kernel, out_shape=jax.ShapeDtypeStruct((ROWS, 256), BF16),...  92.3 us

profile of v6, /device:TPU:1, one launch (start us, length us, event | category | flops | bytes accessed | tf_op | source)
XLA Modules:
  0.0 94.2 jit_solution(16681827850462609021)
XLA Ops:
  0.0 92.3 %shard_map.136 = bf16[1024,256]{1,0:T(8,128)(2,1)} custom-call(bf16[1024,2048]{1,0:T(8,128)(2,1)} %tok_h.1, bf16[128,128]{1,0:T(8,128)(2,1)} %gate_h.1, bf16[128,128]{1,0:T(8,128)(2,1)} %value_h.1, bf16[128,128]{1,0:T(8,128)(2,1)} %mo_h.1, bf16[704,128]{1,0:T(8,128)(2,1)} %bitcast.5, bf16[704,128]{1,0:T(8,128)(2,1)} %bitcast.6, bf16[704,128]{1,0:T(8,128)(2,1)} %wd_h.1, ...), custom_call_target="tpu_custom_call" | custom-call | tf_op jit(solution)/shard_map/pallas_call | solution.py:700
  92.3 1.9 %copy.16 = bf16[1024,256]{1,0:T(8,128)(2,1)} copy(bf16[1024,256]{1,0:T(8,128)(2,1)} %shard_map.136) | data formatting | bytes 1048576

commit v7 on v5

--- a/solution.py
+++ b/solution.py
@@ -375,6 +375,7 @@
     g_wd.step(0)
     g_in1.step(5)
     g_wd.step(1)
+    g_in1.step(3)
     tot[...] = s1.total()
     lane = lax.broadcasted_iota(jnp.int32, (128, 128), 1)
     low = lax.broadcasted_iota(jnp.int32, (128, 128), 0) >= lane
@@ -396,7 +397,6 @@
             def _():
                 r_so.own(part)
 
-    g_in1.step(3)
     g_in2.step(3)
     g_in2.own(first=False)
     r_mo.forward(1)

time: 94.3 us -> 94.3 us (level)
  no operation moved by 1% of the time
where the time goes in v7:
time: 94.3 us; the launch traced here: 94.2 us
  Pallas kernels  92.3 us (98%)
  local copies, waits for them, and re-layouts  1.87 us (2%)
    pallas_call x1, Pallas kernels, per_device(): pl.pallas_call(kernel, out_shape=jax.ShapeDtypeStruct((ROWS, 256), BF16),...  92.3 us

profile of v7, /device:TPU:1, one launch (start us, length us, event | category | flops | bytes accessed | tf_op | source)
XLA Modules:
  0.0 94.2 jit_solution(10344702061284782953)
XLA Ops:
  0.0 92.3 %shard_map.136 = bf16[1024,256]{1,0:T(8,128)(2,1)} custom-call(bf16[1024,2048]{1,0:T(8,128)(2,1)} %tok_h.1, bf16[128,128]{1,0:T(8,128)(2,1)} %gate_h.1, bf16[128,128]{1,0:T(8,128)(2,1)} %value_h.1, bf16[128,128]{1,0:T(8,128)(2,1)} %mo_h.1, bf16[704,128]{1,0:T(8,128)(2,1)} %bitcast.5, bf16[704,128]{1,0:T(8,128)(2,1)} %bitcast.6, bf16[704,128]{1,0:T(8,128)(2,1)} %wd_h.1, ...), custom_call_target="tpu_custom_call" | custom-call | tf_op jit(solution)/shard_map/pallas_call | solution.py:700
  92.3 1.9 %copy.16 = bf16[1024,256]{1,0:T(8,128)(2,1)} copy(bf16[1024,256]{1,0:T(8,128)(2,1)} %shard_map.136) | data formatting | bytes 1048576
